TPU v7x, 256 devices: a whole 4x4x8 slice. The times are simulated.
256 devices in a mesh: sp: 64 (over z, y, core), tp: 4 (over x).
Axes of the slice: x: 4, y: 4, z: 8, core: 2. Of those that a mesh axis runs over, the one named last changes fastest.
Arguments:
- tokens: bfloat16 [4, 24576, 2048], P(None, 'sp'), may hold values from -21 to 21
- query_weight: bfloat16 [2048, 1024], P(None, 'tp'), may hold values from -0.125 to 0.125
- key_weight: bfloat16 [2048, 1024], P(None, 'tp'), may hold values from -0.125 to 0.125
- value_weight: bfloat16 [2048, 1024], P(None, 'tp'), may hold values from -0.125 to 0.125
- out_gain: float32 [1024], replicated, may hold values from 0.1 to 1.9
- out_weight: bfloat16 [1024, 2048], P(None, 'tp'), may hold values from -0.1875 to 0.1875
Outputs:
- mixed_out: bfloat16 [4, 24576, 2048], P(None, 'sp', 'tp')
- total_log: float32 [4, 8, 24576], P(None, 'tp', 'sp')
All inputs are finite; a program needn't handle non-finite values.
Results may differ from a plain program's by a relative error of at most 0.0098.
Values may be sent and summed in bfloat16 or wider, within the bound.
A program may use at most 128 MiB of HBM per device.

v0:
```python
import functools
import math

import jax
import jax.numpy as jnp
import numpy as np
from jax import lax
from jax.experimental import pallas as pl
from jax.experimental.pallas import tpu as pltpu
from jax.sharding import PartitionSpec as P

HEAD_DIM = 128
REACH = 64
FAR = 16
NEAR = 4
GRAN = FAR * FAR
ROPE_BASE = 10000.0
MASK_FILL = -1e30
NORM_FLOOR = 1e-06
LOG2E = 1.0 / math.log(2.0)
LN2 = math.log(2.0)
F32 = jnp.float32
BF16 = jnp.bfloat16

MESH = pl.DeviceIdType.MESH


def iota(shape, dim):
    return lax.broadcasted_iota(jnp.int32, shape, dim)


def perm_token(p):
    slot = p // FAR
    a = p % FAR
    residue = slot // NEAR + NEAR * (slot % (FAR // NEAR))
    return a * FAR + residue


def dot_t(a, b):
    return lax.dot_general(a, b, (((1,), (1,)), ((), ())), preferred_element_type=F32)


def layer_kernel(
    nsp, tok_h, wq_h, wk_h, wv_h, wo_h, cos_h, sin_h, cos_base, sin_base, gain,
    out, log_out,
    tok, wq, wk, wv, wo, cos, sin, kn, qn, kvs, qs, gath, outs, logs, lsend, lrow,
    kp, qp, mp, on, perm, bias1, bias4, bias16, o1, m1, l1,
    load_sem, send_sem, recv_sem,
):
    half = tok.shape[0] // 2
    units = kn.shape[0]
    length = tok.shape[1]
    block = 2 * length
    grans = block // GRAN
    wide = REACH * FAR
    side = wide // GRAN
    tail = wide - block
    span = block + 2 * wide
    rows = block // FAR
    key_rows = span // FAR
    near_rows = rows + 2 * FAR
    cols = wq.shape[1]
    heads = cols // HEAD_DIM
    total = nsp * length
    scale = HEAD_DIM**-0.5 * LOG2E
    sp, t = lax.axis_index("sp"), lax.axis_index("tp")
    y, blk = sp % 2, sp // 2
    twin = sp + 1 - 2 * y
    x_peer = (t + 2) % 4
    d_peer = t + 1 - 2 * (t % 2)
    x_d_peer = (d_peer + 2) % 4
    mine, other = y * half, (1 - y) * half

    loads = []

    def load(src, dst):
        copy = pltpu.make_async_copy(src, dst, load_sem.at[len(loads)])
        copy.start()
        loads.append(copy)
        return copy

    got_cos, got_sin = load(cos_h, cos), load(sin_h, sin)
    got_wk, got_wv = load(wk_h, wk), load(wv_h, wv)
    got_tok = {("m", 0): load(tok_h.at[mine], tok.at[0])}

    barrier = pltpu.get_barrier_semaphore()
    has = {d: (sp + d >= 0) & (sp + d < nsp) for d in (2, -2, 4, -4)}
    reach = {d: has[d] & has[-d] for d in (2, -2)}
    for peer in ((twin, t), (sp, x_peer), (sp, d_peer)):
        pl.semaphore_signal(barrier, inc=1, device_id=peer, device_id_type=MESH)
    count = 3
    for d in (2, -2):
        there = has[d]
        count = count + there.astype(jnp.int32)

        @pl.when(there)
        def _(d=d):
            pl.semaphore_signal(barrier, inc=1, device_id=(sp + d, t), device_id_type=MESH)

    first = pl.multiple_of(y * length, HEAD_DIM)
    second = pl.multiple_of((1 - y) * length, HEAD_DIM)

    def clear(d, at, size):
        @pl.when(jnp.logical_not(has[d]))
        def _():
            for u in range(units):
                kn[u, at : at + size] = jnp.zeros((size, kn.shape[2]), BF16)

    clear(-4, 0, tail)
    clear(-2, tail, block)
    clear(2, wide + block, block)
    clear(4, span - tail, tail)

    numbers = {}

    def copy(name, src, dst, peer):
        n = numbers.setdefault(name, len(numbers))
        return pltpu.make_async_remote_copy(
            src_ref=src, dst_ref=dst, send_sem=send_sem.at[n], recv_sem=recv_sem.at[n],
            device_id=peer, device_id_type=MESH,
        )

    sent = []

    def start(c):
        c.start()
        sent.append((c, None))

    def z_copy(kind, u, d):
        if kind == "T":
            src = wide - tail if d > 0 else wide + block
            dst = 0 if d > 0 else span - tail
            size = tail
        else:
            part = first if kind == "A" else second
            src = wide + part
            dst = (tail if d > 0 else wide + block) + part
            size = length
        return copy(
            (kind, u, d), kn.at[u, pl.ds(src, size)], kn.at[u, pl.ds(dst, size)], (sp + d, t)
        )

    def z_start(kind, u):
        for d in (2, -2):
            c = z_copy(kind, u, d)
            there = reach[d] if kind == "T" else has[d]

            @pl.when(there)
            def _():
                c.start()

            sent.append((c, there))

    def z_wait(kind, u):
        for d in (2, -2):

            @pl.when(has[-2 * d] if kind == "T" else has[-d])
            def _():
                z_copy(kind, u, d).wait_recv()

    def turned(x, w, store):
        a = jnp.dot(x, w[...], preferred_element_type=F32)
        for h in range(heads):
            one = a[:, h * HEAD_DIM : (h + 1) * HEAD_DIM]
            store(h, (one * cos[...] + pltpu.roll(one, HEAD_DIM // 2, 1) * sin[...]).astype(BF16))

    def lanes(n):
        return slice(n * HEAD_DIM, (n + 1) * HEAD_DIM)

    def keys_values(x, put):
        turned(x, wk, lambda h, a: put(2 * h, a))
        v = jnp.dot(x, wv[...], preferred_element_type=F32).astype(BF16)
        for h in range(heads):
            put(2 * h + 1, v[:, lanes(h)])

    def own_kv(s):
        def put(n, a):
            kn[s * heads + n // 2, pl.ds(wide + first, length), lanes(n % 2)] = a

        keys_values(tok[2 * s], put)

    def twin_kv(s):
        def put(n, a):
            kvs[s * heads + n // 2, :, lanes(n % 2)] = a

        keys_values(tok[2 * s + 1], put)

    def own_q(s):
        def put(n, a):
            qn[s * heads + n, pl.ds(first, length)] = a

        turned(tok[2 * s], wq, put)

    def twin_q(s):
        def put(n, a):
            qs[s * heads + n] = a

        turned(tok[2 * s + 1], wq, put)

    def y_kv(u, at):
        return copy(("yk", u), kvs.at[u], kn.at[u, pl.ds(wide + at, length)], (twin, t))

    def y_q(u, at):
        return copy(("yq", u), qs.at[u], qn.at[u, pl.ds(at, length)], (twin, t))

    def of(s):
        return range(s * heads, (s + 1) * heads)

    cos_at, sin_at = cos_base[pl.ds(sp, 1)], sin_base[pl.ds(sp, 1)]
    sign = jnp.where(iota(cos.shape, 1) < HEAD_DIM // 2, -1.0, 1.0)
    got_cos.wait()
    got_sin.wait()
    cos_step, sin_step = cos[...], sin[...]
    cos[...] = cos_step * cos_at - sin_step * sin_at
    sin[...] = (sin_step * cos_at + cos_step * sin_at) * sign
    for c in (got_wk, got_wv, got_tok["m", 0]):
        c.wait()
    got_tok["o", 0] = load(tok_h.at[other], tok.at[1])
    own_kv(0)
    pl.semaphore_wait(barrier, count)
    for u in of(0):
        z_start("A", u)
    got_tok["o", 0].wait()
    got_wq = load(wq_h, wq)
    for s in range(1, half):
        got_tok["o", s] = load(tok_h.at[other + s], tok.at[2 * s + 1])
        got_tok["m", s] = load(tok_h.at[mine + s], tok.at[2 * s])
    got_wo = load(wo_h, wo)
    twin_kv(0)
    for u in of(0):
        start(y_kv(u, first))
    got_wq.wait()
    twin_q(0)
    for u in of(0):
        start(y_q(u, first))
    for s in range(1, half):
        got_tok["o", s].wait()
        got_tok["m", s].wait()
        twin_kv(s)
        for u in of(s):
            start(y_kv(u, first))
        own_kv(s)
    y_kv(0, second).wait_recv()
    z_start("B", 0)
    own_q(0)
    y_kv(1, second).wait_recv()
    z_start("B", 1)
    for s in range(1, half):
        twin_q(s)
        own_q(s)
        for u in of(s):
            start(y_q(u, first))

    perm[...] = jnp.where(
        iota((GRAN, GRAN), 1) == perm_token(iota((GRAN, GRAN), 0)), 1.0, 0.0
    ).astype(BF16)
    origin = blk * block - wide
    shape = (GRAN, GRAN + 2 * REACH)
    token = perm_token(iota(shape, 0))
    for g in range(grans):
        q_at = wide + g * GRAN + token
        k_at = wide + g * GRAN - REACH + iota(shape, 1)
        ok = (jnp.abs(k_at - q_at) <= REACH) & (k_at + origin >= 0) & (k_at + origin < total)
        bias1[g] = jnp.where(ok, 0.0, MASK_FILL)
    per = FAR // NEAR
    shape = (per * rows, per * near_rows)
    row, col = iota(shape, 0), iota(shape, 1)
    q_at = (row % rows + side * FAR) * FAR + NEAR * (row // rows)
    k_at = (col % near_rows + (side - 1) * FAR) * FAR + NEAR * (col // near_rows)
    ok = (jnp.abs(k_at - q_at) <= REACH * NEAR) & (k_at + origin >= 0) & (k_at + origin < total)
    bias4[...] = jnp.where(ok, 0.0, MASK_FILL)
    shape = (rows, key_rows)
    q_at = iota(shape, 0) + side * FAR
    k_at = iota(shape, 1)
    ok = (
        (jnp.abs(k_at - q_at) <= REACH)
        & (k_at * FAR + origin >= 0)
        & (k_at * FAR + origin < total)
    )
    bias16[...] = jnp.where(ok, 0.0, MASK_FILL)

    def gather_keys(u, slot, chunks):
        for j in chunks:
            moved = jnp.dot(
                perm[...], kn[u, j * GRAN : (j + 1) * GRAN], preferred_element_type=F32
            )
            moved = moved.astype(BF16).reshape(FAR, FAR, 2 * HEAD_DIM)
            kp[slot, :, j * FAR : (j + 1) * FAR] = moved

    ends = tail // GRAN

    def attend_close(u):
        slot = u % 2
        y_q(u, second).wait_recv()
        gather_keys(u, slot, range(ends, span // GRAN - ends))
        for g in range(grans):
            moved = jnp.dot(
                perm[...], qn[u, g * GRAN : (g + 1) * GRAN], preferred_element_type=F32
            )
            moved = moved.astype(BF16)
            qp[slot, :, g * FAR : (g + 1) * FAR] = moved.reshape(FAR, FAR, HEAD_DIM)
            at = wide + g * GRAN - REACH
            k = kn[u, at : at + GRAN + 2 * REACH, :HEAD_DIM]
            v = kn[u, at : at + GRAN + 2 * REACH, HEAD_DIM:]
            sc = dot_t(moved, k) * scale + bias1[g]
            m = jnp.max(sc, axis=1, keepdims=True)
            p = jnp.exp2(sc - m)
            l = jnp.sum(p, axis=1, keepdims=True)
            o = jnp.dot(p.astype(BF16), v, preferred_element_type=F32)
            cut = (FAR, FAR, HEAD_DIM)
            o1[slot, :, g * FAR : (g + 1) * FAR] = o.reshape(cut)
            m1[slot, :, g * FAR : (g + 1) * FAR] = jnp.broadcast_to(m, o.shape).reshape(cut)
            l1[slot, :, g * FAR : (g + 1) * FAR] = jnp.broadcast_to(l, o.shape).reshape(cut)

    def attend_far(u):
        slot = u % 2
        s, h = u // heads, u % heads
        z_wait("T", u)
        gather_keys(u, slot, [*range(ends), *range(span // GRAN - ends, span // GRAN)])
        shuffle = perm[...]
        near_at = (side - 1) * FAR
        for group in range(NEAR):
            sel = slice(group * per, (group + 1) * per)
            flat = (per * rows, HEAD_DIM)
            q = qp[slot, sel].reshape(flat)
            k4 = kp[slot, sel, near_at : near_at + near_rows, :HEAD_DIM].reshape(-1, HEAD_DIM)
            v4 = kp[slot, sel, near_at : near_at + near_rows, HEAD_DIM:].reshape(-1, HEAD_DIM)
            s4 = dot_t(q, k4) * scale + bias4[...]
            b16 = bias16[...]
            s16 = jnp.concatenate(
                [
                    dot_t(qp[slot, group * per + i], kp[slot, group * per + i, :, :HEAD_DIM]) * scale + b16
                    for i in range(per)
                ],
                axis=0,
            )
            m_old = m1[slot, sel].reshape(flat)
            m_row = jnp.maximum(
                jnp.max(s4, axis=1, keepdims=True), jnp.max(s16, axis=1, keepdims=True)
            )
            m_new = jnp.maximum(m_old, m_row)
            m_col = m_new[:, :1]
            keep = jnp.exp2(m_old - m_new)
            p4 = jnp.exp2(s4 - m_col)
            p16 = jnp.exp2(s16 - m_col)
            l = l1[slot, sel].reshape(flat) * keep + (
                jnp.sum(p4, axis=1, keepdims=True) + jnp.sum(p16, axis=1, keepdims=True)
            )
            p16 = p16.astype(BF16)
            o16 = jnp.concatenate(
                [
                    jnp.dot(
                        p16[i * rows : (i + 1) * rows],
                        kp[slot, group * per + i, :, HEAD_DIM:],
                        preferred_element_type=F32,
                    )
                    for i in range(per)
                ],
                axis=0,
            )
            o = o1[slot, sel].reshape(flat) * keep + o16
            o = o + jnp.dot(p4.astype(BF16), v4, preferred_element_type=F32)
            mp[sel] = (o / l).astype(BF16).reshape(per, rows, HEAD_DIM)
            m1[slot, sel] = (m_new * LN2 + jnp.log(l)).reshape(per, rows, HEAD_DIM)
        lane = iota((GRAN, HEAD_DIM), 1)
        for g in range(grans):
            cut = slice(g * FAR, (g + 1) * FAR)
            back = lambda a: lax.dot_general(
                a, shuffle, (((0,), (0,)), ((), ())), preferred_element_type=F32
            )
            merged = lax.dot_general(
                shuffle,
                mp[:, cut].reshape(GRAN, HEAD_DIM),
                (((0,), (0,)), ((), ())),
                preferred_element_type=F32,
            )
            on[g * GRAN : (g + 1) * GRAN] = merged.astype(BF16)
            x = m1[slot, :, cut].reshape(GRAN, HEAD_DIM)
            high = x.astype(BF16).astype(F32)
            mid = (x - high).astype(BF16).astype(F32)
            low = x - high - mid
            terms = jnp.where(
                lane == 0, high, jnp.where(lane == 1, mid, jnp.where(lane == 2, low, 0.0))
            )
            lrow[:, g * GRAN : (g + 1) * GRAN] = jnp.sum(
                back(terms.astype(BF16)), axis=0, keepdims=True
            )
        outs[u] = on[pl.ds(second, length)]
        gath[t, mine + s, h] = on[pl.ds(first, length)]
        logs[mine + s, h] = lrow[:, pl.ds(first, length)]
        lsend[u] = lrow[:, pl.ds(second, length)]
        start(across(u, mine))
        start(piece("xm", u, t, mine, (sp, x_peer)))
        start(piece("dm", u, t, mine, (sp, d_peer)))
        start(log_across(u, mine))

    def across(u, base):
        return copy(
            ("yo", u), outs.at[u], gath.at[t, base + u // heads, u % heads], (twin, t)
        )

    def log_across(u, base):
        return copy(("yl", u), lsend.at[u], logs.at[base + u // heads, u % heads], (twin, t))

    def piece(name, u, owner, base, peer):
        ref = gath.at[owner, base + u // heads, u % heads]
        return copy((name, u), ref, ref, peer)

    def spread(u):
        across(u, other).wait_recv()
        start(piece("xr", u, t, other, (sp, x_peer)))
        start(piece("dr", u, t, other, (sp, d_peer)))
        piece("xm", u, x_peer, mine, (sp, x_peer)).wait_recv()
        start(piece("em", u, x_peer, mine, (sp, d_peer)))

    def spread_twin(u):
        piece("xr", u, x_peer, other, (sp, x_peer)).wait_recv()
        start(piece("er", u, x_peer, other, (sp, d_peer)))
        log_across(u, other).wait_recv()

    def finish(j):
        acc = None
        square = None
        for n in range(gath.shape[0]):
            x = jnp.concatenate([gath[n, j, h] for h in range(heads)], axis=1).astype(F32)
            at = slice(n * cols, (n + 1) * cols)
            scaled = (x * gain[:, at]).astype(BF16)
            term = jnp.dot(scaled, wo[at], preferred_element_type=F32)
            sq = jnp.sum(x * x, axis=1, keepdims=True)
            acc = term if acc is None else acc + term
            square = sq if square is None else square + sq
        out[j] = (acc * lax.rsqrt(square / wo.shape[0] + NORM_FLOOR)).astype(BF16)

    def finish_mine(s):
        for u in of(s):
            piece("dm", u, d_peer, mine, (sp, d_peer)).wait_recv()
            piece("em", u, x_d_peer, mine, (sp, d_peer)).wait_recv()
        finish(mine + s)

    def finish_other(s):
        for u in of(s):
            piece("dr", u, d_peer, other, (sp, d_peer)).wait_recv()
            piece("er", u, x_d_peer, other, (sp, d_peer)).wait_recv()
        finish(other + s)

    def arrived(u):
        z_wait("A", u)
        z_wait("B", u)

    arrived(0)
    z_start("T", 0)
    z_start("A", 2)
    arrived(1)
    z_start("T", 1)
    y_kv(2, second).wait_recv()
    z_start("B", 2)
    z_start("A", 3)
    attend_close(0)
    attend_far(0)
    attend_close(1)
    attend_far(1)
    arrived(2)
    z_start("T", 2)
    y_kv(3, second).wait_recv()
    z_start("B", 3)
    spread(0)
    spread(1)
    attend_close(2)
    spread_twin(0)
    spread_twin(1)
    got_wo.wait()
    arrived(3)
    z_start("T", 3)
    attend_close(3)
    attend_far(2)
    finish_mine(0)
    spread(2)
    attend_far(3)
    spread_twin(2)
    finish_other(0)
    spread(3)
    finish_mine(1)
    spread_twin(3)
    finish_other(1)
    for j in range(logs.shape[0]):
        for h in range(heads):
            log_out[j, h : h + 1] = logs[j, h]
    for c, there in sent:
        if there is None:
            c.wait_send()
        else:

            @pl.when(there)
            def _(c=c):
                c.wait_send()


def layer(nsp, ntp, tokens, wq, wk, wv, wo, tables, gain):
    seqs, length, width = tokens.shape
    half = seqs // 2
    cols = wq.shape[1]
    heads = cols // HEAD_DIM
    block = 2 * length
    wide = REACH * FAR
    span = block + 2 * wide
    rows = block // FAR
    near_rows = rows + 2 * FAR
    per = FAR // NEAR
    grans = block // GRAN
    hbm = pl.BlockSpec(memory_space=pl.ANY)
    vmem = pl.BlockSpec(memory_space=pltpu.VMEM)
    v = pltpu.VMEM
    return pl.pallas_call(
        functools.partial(layer_kernel, nsp),
        in_specs=[hbm] * 7 + [vmem] * 3,
        out_specs=[vmem, vmem],
        out_shape=[
            jax.ShapeDtypeStruct((seqs, length, wo.shape[1]), BF16),
            jax.ShapeDtypeStruct((seqs, heads, length), F32),
        ],
        scratch_shapes=[
            v(tokens.shape, BF16), v(wq.shape, BF16), v(wk.shape, BF16), v(wv.shape, BF16),
            v(wo.shape, BF16), v((length, HEAD_DIM), F32), v((length, HEAD_DIM), F32),
            v((half * heads, span, 2 * HEAD_DIM), BF16),
            v((half * heads, block, HEAD_DIM), BF16),
            v((half * heads, length, 2 * HEAD_DIM), BF16),
            v((half * heads, length, HEAD_DIM), BF16),
            v((ntp, seqs, heads, length, HEAD_DIM), BF16),
            v((half * heads, length, HEAD_DIM), BF16),
            v((seqs, heads, 1, length), F32),
            v((half * heads, 1, length), F32),
            v((1, block), F32),
            v((2, FAR, span // FAR, 2 * HEAD_DIM), BF16),
            v((2, FAR, rows, HEAD_DIM), BF16),
            v((FAR, rows, HEAD_DIM), BF16),
            v((block, HEAD_DIM), BF16),
            v((GRAN, GRAN), BF16),
            v((grans, GRAN, GRAN + 2 * REACH), F32),
            v((per * rows, per * near_rows), F32),
            v((rows, span // FAR), F32),
            v((2, FAR, rows, HEAD_DIM), F32),
            v((2, FAR, rows, HEAD_DIM), F32),
            v((2, FAR, rows, HEAD_DIM), F32),
            pltpu.SemaphoreType.DMA((seqs + 6,)),
            pltpu.SemaphoreType.DMA((16 * half * heads,)),
            pltpu.SemaphoreType.DMA((16 * half * heads,)),
        ],
        compiler_params=pltpu.CompilerParams(
            collective_id=0, has_side_effects=True, vmem_limit_bytes=56 * 2**20
        ),
        name="layer",
    )(tokens, wq, wk, wv, wo, *tables, gain)


def shards(tokens, query_weight, key_weight, value_weight, out_gain, out_weight):
    length = tokens.shape[1]
    nsp = lax.axis_size("sp")
    frequency = ROPE_BASE ** (-np.arange(HEAD_DIM // 2) / (HEAD_DIM // 2))
    frequency = np.tile(frequency, 2)[None, :]
    step = np.arange(length)[:, None] * frequency
    base = (np.arange(nsp) * length)[:, None] * frequency
    tables = [
        jnp.asarray(f(a).astype(np.float32)) for a in (step, base) for f in (np.cos, np.sin)
    ]
    return tuple(
        layer(
            nsp, lax.axis_size("tp"), tokens, query_weight, key_weight, value_weight,
            out_weight, tables, out_gain[None, :],
        )
    )


def solution(mesh):
    return jax.shard_map(
        shards,
        mesh=mesh,
        in_specs=(
            P(None, "sp", None),
            P(None, "tp"),
            P(None, "tp"),
            P(None, "tp"),
            P(),
            P(None, "tp"),
        ),
        out_specs=(P(None, "sp", "tp"), P(None, "tp", "sp")),
        check_vma=False,
    )
```

profile of v0, /device:TPU:160, one launch (start us, length us, event | category | flops | bytes accessed | tf_op | source)
XLA Modules:
  0.0 95.0 jit_solution(6727421644436402992)
XLA Ops:
  0.6 91.1 %layer.1 = (bf16[4,384,512]{2,1,0:T(8,128)(2,1)}, f32[4,2,384]{2,1,0:T(2,128)}) custom-call(bf16[4,384,2048]{2,1,0:T(8,128)(2,1)} %tok_h.1, bf16[2048,256]{1,0:T(8,128)(2,1)} %wq_h.1, bf16[2048,256]{1,0:T(8,128)(2,1)} %wk_h.1, bf16[2048,256]{1,0:T(8,128)(2,1)} %wv_h.1, bf16[1024,512]{1,0:T(8,128)(2,1)} %wo_h.1, f32[384,128]{1,0:T(8,128)} %constant.8.clone.cos_h, ...), custom_call_target="tpu_custom_call" | custom-call | tf_op jit(solution)/shard_map/layer/pallas_call | solution.py:513
  91.7 0.0 copy-start
  91.7 2.7 %copy.14 = bf16[4,384,512]{2,1,0:T(8,128)(2,1)} copy(bf16[4,384,512]{2,1,0:T(8,128)(2,1)} %get-tuple-element.4) | data formatting | bytes 3145728
  94.4 0.0 copy-done
  94.4 0.6 copy.15
Async XLA Ops:
  91.7 2.7 %copy-start = (f32[4,2,384]{2,1,0:T(2,128)S(1)}, f32[4,2,384]{2,1,0:T(2,128)}, u32[]{:S(2)}) copy-start(f32[4,2,384]{2,1,0:T(2,128)} %get-tuple-element.5) | copy-start | bytes 36868
where the time goes:
time: 95.2 us; the launch traced here: 95 us
  Pallas kernels  91.1 us (96%)
  local copies, waits for them, and re-layouts  3.26 us (3%)
    pallas_call x1, Pallas kernels, layer(): pl.pallas_call(functools.partial(layer_kernel, nsp), in_specs=[hbm] * 7 +...  91.1 us
    unnamed x4, local copies, waits for them, and re-layouts  3.26 us

commit v1 on v0

--- a/solution.py
+++ b/solution.py
@@ -66,9 +66,7 @@
     sp, t = lax.axis_index("sp"), lax.axis_index("tp")
     y, blk = sp % 2, sp // 2
     twin = sp + 1 - 2 * y
-    x_peer = (t + 2) % 4
-    d_peer = t + 1 - 2 * (t % 2)
-    x_d_peer = (d_peer + 2) % 4
+    right, left, opposite = (t + 1) % 4, (t + 3) % 4, (t + 2) % 4
     mine, other = y * half, (1 - y) * half
 
     loads = []
@@ -86,7 +84,7 @@
     barrier = pltpu.get_barrier_semaphore()
     has = {d: (sp + d >= 0) & (sp + d < nsp) for d in (2, -2, 4, -4)}
     reach = {d: has[d] & has[-d] for d in (2, -2)}
-    for peer in ((twin, t), (sp, x_peer), (sp, d_peer)):
+    for peer in ((twin, t), (sp, right), (sp, left)):
         pl.semaphore_signal(barrier, inc=1, device_id=peer, device_id_type=MESH)
     count = 3
     for d in (2, -2):
@@ -390,8 +388,8 @@
         logs[mine + s, h] = lrow[:, pl.ds(first, length)]
         lsend[u] = lrow[:, pl.ds(second, length)]
         start(across(u, mine))
-        start(piece("xm", u, t, mine, (sp, x_peer)))
-        start(piece("dm", u, t, mine, (sp, d_peer)))
+        start(piece("mr", u, t, mine, right))
+        start(piece("ml", u, t, mine, left))
         start(log_across(u, mine))
 
     def across(u, base):
@@ -402,20 +400,20 @@
     def log_across(u, base):
         return copy(("yl", u), lsend.at[u], logs.at[base + u // heads, u % heads], (twin, t))
 
-    def piece(name, u, owner, base, peer):
+    def piece(name, u, owner, base, to):
         ref = gath.at[owner, base + u // heads, u % heads]
-        return copy((name, u), ref, ref, peer)
+        return copy((name, u), ref, ref, (sp, to))
 
     def spread(u):
         across(u, other).wait_recv()
-        start(piece("xr", u, t, other, (sp, x_peer)))
-        start(piece("dr", u, t, other, (sp, d_peer)))
-        piece("xm", u, x_peer, mine, (sp, x_peer)).wait_recv()
-        start(piece("em", u, x_peer, mine, (sp, d_peer)))
+        start(piece("or", u, t, other, right))
+        start(piece("ol", u, t, other, left))
+        piece("mr", u, left, mine, right).wait_recv()
+        start(piece("fr", u, left, mine, right))
 
     def spread_twin(u):
-        piece("xr", u, x_peer, other, (sp, x_peer)).wait_recv()
-        start(piece("er", u, x_peer, other, (sp, d_peer)))
+        piece("ol", u, right, other, left).wait_recv()
+        start(piece("fl", u, right, other, left))
         log_across(u, other).wait_recv()
 
     def finish(j):
@@ -433,14 +431,14 @@
 
     def finish_mine(s):
         for u in of(s):
-            piece("dm", u, d_peer, mine, (sp, d_peer)).wait_recv()
-            piece("em", u, x_d_peer, mine, (sp, d_peer)).wait_recv()
+            piece("ml", u, right, mine, left).wait_recv()
+            piece("fr", u, opposite, mine, right).wait_recv()
         finish(mine + s)
 
     def finish_other(s):
         for u in of(s):
-            piece("dr", u, d_peer, other, (sp, d_peer)).wait_recv()
-            piece("er", u, x_d_peer, other, (sp, d_peer)).wait_recv()
+            piece("or", u, left, other, right).wait_recv()
+            piece("fl", u, opposite, other, left).wait_recv()
         finish(other + s)
 
     def arrived(u):

time: 95.2 us -> 82.4 us (0.87)
  Pallas kernels: 91.1 us -> 78.3 us
    pallas_call x1, Pallas kernels: 91.1 us -> 78.3 us  [layer(): pl.pallas_call(functools.partial(layer_kernel, nsp), in_specs=[hbm] * 7 +...]
where the time goes in v1:
time: 82.4 us; the launch traced here: 82.2 us
  Pallas kernels  78.3 us (95%)
  local copies, waits for them, and re-layouts  3.26 us (4%)
    pallas_call x1, Pallas kernels, layer(): pl.pallas_call(functools.partial(layer_kernel, nsp), in_specs=[hbm] * 7 +...  78.3 us
    unnamed x4, local copies, waits for them, and re-layouts  3.26 us

profile of v1, /device:TPU:160, one launch (start us, length us, event | category | flops | bytes accessed | tf_op | source)
XLA Modules:
  0.0 82.2 jit_solution(17179526445422106958)
XLA Ops:
  0.6 78.3 %layer.1 = (bf16[4,384,512]{2,1,0:T(8,128)(2,1)}, f32[4,2,384]{2,1,0:T(2,128)}) custom-call(bf16[4,384,2048]{2,1,0:T(8,128)(2,1)} %tok_h.1, bf16[2048,256]{1,0:T(8,128)(2,1)} %wq_h.1, bf16[2048,256]{1,0:T(8,128)(2,1)} %wk_h.1, bf16[2048,256]{1,0:T(8,128)(2,1)} %wv_h.1, bf16[1024,512]{1,0:T(8,128)(2,1)} %wo_h.1, f32[384,128]{1,0:T(8,128)} %constant.8.clone.cos_h, ...), custom_call_target="tpu_custom_call" | custom-call | tf_op jit(solution)/shard_map/layer/pallas_call | solution.py:511
  78.9 0.0 copy-start
  78.9 2.7 %copy.14 = bf16[4,384,512]{2,1,0:T(8,128)(2,1)} copy(bf16[4,384,512]{2,1,0:T(8,128)(2,1)} %get-tuple-element.4) | data formatting | bytes 3145728
  81.6 0.0 copy-done
  81.6 0.6 copy.15
Async XLA Ops:
  78.9 2.7 %copy-start = (f32[4,2,384]{2,1,0:T(2,128)S(1)}, f32[4,2,384]{2,1,0:T(2,128)}, u32[]{:S(2)}) copy-start(f32[4,2,384]{2,1,0:T(2,128)} %get-tuple-element.5) | copy-start | bytes 36868

commit v2 on v1

v2 whole, which is shorter than its diff:
```python
import functools
import math

import jax
import jax.numpy as jnp
import numpy as np
from jax import lax
from jax.experimental import pallas as pl
from jax.experimental.pallas import tpu as pltpu
from jax.sharding import PartitionSpec as P

HEAD_DIM = 128
REACH = 64
FAR = 16
NEAR = 4
GRAN = FAR * FAR
ROPE_BASE = 10000.0
MASK_FILL = -1e30
NORM_FLOOR = 1e-06
LOG2E = 1.0 / math.log(2.0)
LN2 = math.log(2.0)
F32 = jnp.float32
BF16 = jnp.bfloat16

MESH = pl.DeviceIdType.MESH


def iota(shape, dim):
    return lax.broadcasted_iota(jnp.int32, shape, dim)


def perm_token(p):
    slot = p // FAR
    a = p % FAR
    residue = slot // NEAR + NEAR * (slot % (FAR // NEAR))
    return a * FAR + residue


def dot_t(a, b):
    return lax.dot_general(a, b, (((1,), (1,)), ((), ())), preferred_element_type=F32)


def layer_kernel(
    nsp, tok_h, wq_h, wk_h, wv_h, wo_h, cos_h, sin_h, cos_base, sin_base, gain,
    out, log_out,
    tok, wq, wk, wv, wo, cos, sin, kn, qn, kvs, qs, gath, outs, logs, lsend,
    kp, qp, mp, perm, bias1, bias4, bias16, o1, m1, l1, acc, sq,
    load_sem, send_sem, recv_sem,
):
    seqs, length = tok.shape[:2]
    block = 2 * length
    grans = block // GRAN
    wide = REACH * FAR
    side = wide // GRAN
    own = seqs // 2 * block
    span = own + 2 * wide
    window = block + 2 * wide
    rows = block // FAR
    key_rows = window // FAR
    near_rows = rows + 2 * FAR
    cols = wq.shape[1]
    heads = cols // HEAD_DIM
    total = nsp * length
    scale = HEAD_DIM**-0.5 * LOG2E
    sp, t = lax.axis_index("sp"), lax.axis_index("tp")
    plane = 2 * seqs
    z, y, c = sp // plane, (sp // 2) % seqs, sp % 2
    worker = y // 2
    mine = worker == c
    place = 2 * (y % 2) + c
    right, left, opposite = (t + 1) % 4, (t + 3) % 4, (t + 2) % 4
    part = 2 * z + c
    last = 2 * (nsp // plane) - 1
    above, below = part < last, part > 0

    def at(zz, yy, cc):
        return (zz * plane + yy * 2 + cc, t)

    def half_at(p):
        return at(p // 2, y, p % 2)

    def seq(k):
        return (y + k) % seqs

    loads = []

    def load(src, dst):
        copy = pltpu.make_async_copy(src, dst, load_sem.at[len(loads)])
        copy.start()
        loads.append(copy)
        return copy

    order = (1, 3, 2, 0)
    got_cos, got_sin = load(cos_h, cos), load(sin_h, sin)
    got_wk, got_wv = load(wk_h, wk), load(wv_h, wv)
    got_tok = {}
    for k in order[:1]:
        got_tok[k] = load(tok_h.at[seq(k)], tok.at[k])

    barrier = pltpu.get_barrier_semaphore()

    def greet(peer):
        pl.semaphore_signal(barrier, inc=1, device_id=peer, device_id_type=MESH)

    for k in range(1, seqs):
        greet(at(z, seq(k), worker))
    for i in range(2):
        for cc in range(2):

            @pl.when(jnp.logical_not((2 * c + i == y) & (cc == c)))
            def _(i=i, cc=cc):
                greet(at(z, 2 * c + i, cc))

    @pl.when(jnp.logical_not(mine))
    def _():
        greet(at(z, y, worker))

    greet((sp, right))
    greet((sp, left))

    @pl.when(above)
    def _():
        greet(half_at(part + 1))

    @pl.when(below)
    def _():
        greet(half_at(part - 1))

    count = (
        2 * seqs + 2 - 2 * mine.astype(jnp.int32)
        + above.astype(jnp.int32) + below.astype(jnp.int32)
    )

    @pl.when(jnp.logical_not(below))
    def _():
        for h in range(heads):
            kn[h, 0:wide] = jnp.zeros((wide, kn.shape[2]), BF16)

    @pl.when(jnp.logical_not(above))
    def _():
        for h in range(heads):
            kn[h, wide + own : span] = jnp.zeros((wide, kn.shape[2]), BF16)

    def copy(src, dst, send, recv, peer):
        return pltpu.make_async_remote_copy(
            src_ref=src, dst_ref=dst, send_sem=send_sem.at[send], recv_sem=recv_sem.at[recv],
            device_id=peer, device_id_type=MESH,
        )

    sent = []

    def start(c, there=None):
        if there is None:
            c.start()
        else:

            @pl.when(there)
            def _():
                c.start()

        sent.append((c, there))

    def unless(cond, c):
        @pl.when(jnp.logical_not(cond))
        def _():
            c.wait_recv()

    def chunk(j):
        return pl.ds(pl.multiple_of(wide + j * length, HEAD_DIM), length)

    def q_chunk(j):
        return pl.ds(pl.multiple_of(j * length, HEAD_DIM), length)

    def kv_copy(h, k, j):
        return copy(
            kvs.at[k * heads + h], kn.at[h, chunk(j)], h * 4 + k, h * 4 + j,
            at(z, seq(k), worker),
        )

    def q_copy(h, k, j):
        return copy(
            qs.at[k * heads + h], qn.at[h, q_chunk(j)], 8 + h * 4 + k, 8 + h * 4 + j,
            at(z, seq(k), worker),
        )

    def is_here(j):
        return (2 * c + j // 2 == y) & (j % 2 == c)

    def kv_send(h, k):
        if k == 0:

            @pl.when(mine)
            def _():
                kn[h, chunk(place)] = kvs[h]

        start(kv_copy(h, k, place), jnp.logical_not(mine) if k == 0 else None)

    def q_send(h, k):
        if k == 0:

            @pl.when(mine)
            def _():
                qn[h, q_chunk(place)] = qs[h]

        start(q_copy(h, k, place), jnp.logical_not(mine) if k == 0 else None)

    first_up = wide + own - wide
    cuts_up = [(first_up, 2 * length - (own - wide)), (wide + 2 * length, length), (wide + 3 * length, length)]
    cuts_down = [(wide, length), (wide + length, length), (wide + 2 * length, wide - 2 * length)]

    def up(h, p):
        row, size = cuts_up[p]
        return copy(
            kn.at[h, row : row + size], kn.at[h, row - own : row - own + size],
            16 + 3 * h + p, 16 + 3 * h + p, half_at(part + 1),
        )

    def down(h, p):
        row, size = cuts_down[p]
        return copy(
            kn.at[h, row : row + size], kn.at[h, row + own : row + own + size],
            22 + 3 * h + p, 22 + 3 * h + p, half_at(part - 1),
        )

    def forward(h):
        for j in range(4):
            unless(is_here(j), kv_copy(h, 0, j))
            if j < 3:
                start(down(h, j), below)
            if j > 0:
                start(up(h, j - 1), above)

    def halo(h):
        for p in range(3):
            unless(jnp.logical_not(below), up(h, p))
            unless(jnp.logical_not(above), down(h, p))

    def lanes(n):
        return slice(n * HEAD_DIM, (n + 1) * HEAD_DIM)

    def turned(x, w, store):
        a = jnp.dot(x, w[...], preferred_element_type=F32)
        for h in range(heads):
            one = a[:, lanes(h)]
            store(h, (one * cos[...] + pltpu.roll(one, HEAD_DIM // 2, 1) * sin[...]).astype(BF16))

    def project_kv(k):
        x = tok[k]

        def put(h, a):
            kvs[k * heads + h, :, :HEAD_DIM] = a

        turned(x, wk, put)
        v = jnp.dot(x, wv[...], preferred_element_type=F32).astype(BF16)
        for h in range(heads):
            kvs[k * heads + h, :, HEAD_DIM:] = v[:, lanes(h)]

    def project_q(k):
        def put(h, a):
            qs[k * heads + h] = a

        turned(tok[k], wq, put)

    cos_at, sin_at = cos_base[pl.ds(sp, 1)], sin_base[pl.ds(sp, 1)]
    sign = jnp.where(iota(cos.shape, 1) < HEAD_DIM // 2, -1.0, 1.0)
    got_cos.wait()
    got_sin.wait()
    cos_step, sin_step = cos[...], sin[...]
    cos[...] = cos_step * cos_at - sin_step * sin_at
    sin[...] = (sin_step * cos_at + cos_step * sin_at) * sign
    for c_ in (got_wk, got_wv, got_tok[order[0]]):
        c_.wait()
    for k in order[1:]:
        got_tok[k] = load(tok_h.at[seq(k)], tok.at[k])
    got_wq = load(wq_h, wq)
    got_wo = load(wo_h, wo)
    project_kv(order[0])
    pl.semaphore_wait(barrier, count)
    kv_send(0, order[0])
    for k in order[1:]:
        got_tok[k].wait()
        project_kv(k)
        kv_send(0, k)
    got_wq.wait()
    for k in order:
        project_q(k)
        q_send(0, k)
    for k in order:
        kv_send(1, k)
    for k in order:
        q_send(1, k)

    perm[...] = jnp.where(
        iota((GRAN, GRAN), 1) == perm_token(iota((GRAN, GRAN), 0)), 1.0, 0.0
    ).astype(BF16)
    per = FAR // NEAR
    for jb in range(2):
        origin = part * own - wide + jb * block
        shape = (GRAN, GRAN + 2 * REACH)
        token = perm_token(iota(shape, 0))
        for g in range(grans):
            q_at = wide + g * GRAN + token
            k_at = wide + g * GRAN - REACH + iota(shape, 1)
            ok = (jnp.abs(k_at - q_at) <= REACH) & (k_at + origin >= 0) & (k_at + origin < total)
            bias1[jb, g] = jnp.where(ok, 0.0, MASK_FILL)
        shape = (per * rows, per * near_rows)
        row, col = iota(shape, 0), iota(shape, 1)
        q_at = (row % rows + side * FAR) * FAR + NEAR * (row // rows)
        k_at = (col % near_rows + (side - 1) * FAR) * FAR + NEAR * (col // near_rows)
        ok = (jnp.abs(k_at - q_at) <= REACH * NEAR) & (k_at + origin >= 0) & (k_at + origin < total)
        bias4[jb] = jnp.where(ok, 0.0, MASK_FILL)
        shape = (rows, key_rows)
        q_at = iota(shape, 0) + side * FAR
        k_at = iota(shape, 1)
        ok = (
            (jnp.abs(k_at - q_at) <= REACH)
            & (k_at * FAR + origin >= 0)
            & (k_at * FAR + origin < total)
        )
        bias16[jb] = jnp.where(ok, 0.0, MASK_FILL)

    def gather_keys(h, chunks):
        for j in chunks:
            moved = jnp.dot(
                perm[...], kn[h, j * GRAN : (j + 1) * GRAN], preferred_element_type=F32
            )
            moved = moved.astype(BF16).reshape(FAR, FAR, 2 * HEAD_DIM)
            kp[h, :, j * FAR : (j + 1) * FAR] = moved

    def ready(h):
        gather_keys(h, range(side, (wide + own) // GRAN))
        for j in range(4):
            unless(is_here(j), q_copy(h, 0, j))
        halo(h)
        gather_keys(h, [*range(side), *range((wide + own) // GRAN, span // GRAN)])

    def attend_close(h, step):
        slot = step
        jb = (step + y) % 2
        off = jb * block
        for g in range(grans):
            moved = jnp.dot(
                perm[...],
                qn[h, pl.ds(pl.multiple_of(off + g * GRAN, GRAN), GRAN)],
                preferred_element_type=F32,
            )
            moved = moved.astype(BF16)
            qp[slot, :, g * FAR : (g + 1) * FAR] = moved.reshape(FAR, FAR, HEAD_DIM)
            near = pl.ds(
                pl.multiple_of(off + wide + g * GRAN - REACH, REACH), GRAN + 2 * REACH
            )
            k = kn[h, near, :HEAD_DIM]
            v = kn[h, near, HEAD_DIM:]
            sc = dot_t(moved, k) * scale + bias1[jb, g]
            m = jnp.max(sc, axis=1, keepdims=True)
            p = jnp.exp2(sc - m)
            l = jnp.sum(p, axis=1, keepdims=True)
            o = jnp.dot(p.astype(BF16), v, preferred_element_type=F32)
            cut = (FAR, FAR, HEAD_DIM)
            o1[slot, :, g * FAR : (g + 1) * FAR] = o.reshape(cut)
            m1[slot, :, g * FAR : (g + 1) * FAR] = jnp.broadcast_to(m, o.shape).reshape(cut)
            l1[slot, :, g * FAR : (g + 1) * FAR] = jnp.broadcast_to(l, o.shape).reshape(cut)

    def attend_far(h, step):
        slot = step
        hs = 2 * h + step
        jb = (step + y) % 2
        shuffle = perm[...]
        near = pl.ds(pl.multiple_of((side - 1) * FAR + jb * rows, FAR), near_rows)
        whole = pl.ds(pl.multiple_of(jb * rows, FAR), key_rows)
        for group in range(NEAR):
            sel = slice(group * per, (group + 1) * per)
            flat = (per * rows, HEAD_DIM)
            q = qp[slot, sel].reshape(flat)
            k4 = kp[h, sel, near, :HEAD_DIM].reshape(-1, HEAD_DIM)
            v4 = kp[h, sel, near, HEAD_DIM:].reshape(-1, HEAD_DIM)
            s4 = dot_t(q, k4) * scale + bias4[jb]
            b16 = bias16[jb]
            s16 = jnp.concatenate(
                [
                    dot_t(qp[slot, group * per + i], kp[h, group * per + i, whole, :HEAD_DIM]) * scale + b16
                    for i in range(per)
                ],
                axis=0,
            )
            m_old = m1[slot, sel].reshape(flat)
            m_row = jnp.maximum(
                jnp.max(s4, axis=1, keepdims=True), jnp.max(s16, axis=1, keepdims=True)
            )
            m_new = jnp.maximum(m_old, m_row)
            m_col = m_new[:, :1]
            keep = jnp.exp2(m_old - m_new)
            p4 = jnp.exp2(s4 - m_col)
            p16 = jnp.exp2(s16 - m_col)
            l = l1[slot, sel].reshape(flat) * keep + (
                jnp.sum(p4, axis=1, keepdims=True) + jnp.sum(p16, axis=1, keepdims=True)
            )
            p16 = p16.astype(BF16)
            o16 = jnp.concatenate(
                [
                    jnp.dot(
                        p16[i * rows : (i + 1) * rows],
                        kp[h, group * per + i, whole, HEAD_DIM:],
                        preferred_element_type=F32,
                    )
                    for i in range(per)
                ],
                axis=0,
            )
            o = o1[slot, sel].reshape(flat) * keep + o16
            o = o + jnp.dot(p4.astype(BF16), v4, preferred_element_type=F32)
            mp[slot, sel] = (o / l).astype(BF16).reshape(per, rows, HEAD_DIM)
            m1[slot, sel] = (m_new * LN2 + jnp.log(l)).reshape(per, rows, HEAD_DIM)
        lane = iota((GRAN, HEAD_DIM), 1)
        for g in range(grans):
            cut = slice(g * FAR, (g + 1) * FAR)
            back = lambda a: lax.dot_general(
                a, shuffle, (((0,), (0,)), ((), ())), preferred_element_type=F32
            )
            merged = lax.dot_general(
                shuffle,
                mp[slot, :, cut].reshape(GRAN, HEAD_DIM),
                (((0,), (0,)), ((), ())),
                preferred_element_type=F32,
            )
            outs[hs, g * GRAN : (g + 1) * GRAN] = merged.astype(BF16)
            x = m1[slot, :, cut].reshape(GRAN, HEAD_DIM)
            high = x.astype(BF16).astype(F32)
            mid = (x - high).astype(BF16).astype(F32)
            low = x - high - mid
            terms = jnp.where(
                lane == 0, high, jnp.where(lane == 1, mid, jnp.where(lane == 2, low, 0.0))
            )
            lsend[hs, :, g * GRAN : (g + 1) * GRAN] = jnp.sum(
                back(terms.astype(BF16)), axis=0, keepdims=True
            )
        for cc in range(2):
            home = 2 * c + jb
            here = (home == y) & (cc == c)
            cut = slice(cc * length, (cc + 1) * length)

            @pl.when(here)
            def _(cut=cut):
                gath[t, y, h] = outs[hs, cut]
                logs[y, h] = lsend[hs, :, cut]

            start(o_copy(h, y, outs.at[hs, cut], 2 * hs + cc, at(z, home, cc)), jnp.logical_not(here))
            start(l_copy(h, y, lsend.at[hs, :, cut], 2 * hs + cc, at(z, home, cc)), jnp.logical_not(here))

    def o_copy(h, s, src, n, peer):
        return copy(src, gath.at[t, s, h], 28 + n, 28 + 2 * s + h, peer)

    def l_copy(h, s, src, n, peer):
        return copy(src, logs.at[s, h], 36 + n, 36 + 2 * s + h, peer)

    def piece(kind, h, k, owner, to):
        ref = gath.at[owner, seq(k), h]
        n = 44 + 8 * kind + 2 * k + h
        return copy(ref, ref, n, n, (sp, to))

    def collect(h, k):
        w = o_copy(h, seq(k), outs.at[0, :length], 0, (sp, right))
        if k == 0:
            unless(mine, w)
        else:
            w.wait_recv()
        start(piece(0, h, k, t, right))
        start(piece(1, h, k, t, left))

    def relay(h, k):
        if k in (0, 1):
            piece(0, h, k, left, right).wait_recv()
            start(piece(2, h, k, left, right))
        else:
            piece(1, h, k, right, left).wait_recv()
            start(piece(2, h, k, right, left))

    def rest(h, k):
        if k in (0, 1):
            piece(1, h, k, right, left).wait_recv()
        else:
            piece(0, h, k, left, right).wait_recv()
        piece(2, h, k, opposite, right).wait_recv()

    def share(h, k):
        term, square = None, None
        s = seq(k)
        x = jnp.concatenate([gath[n, s, h] for n in range(4)], axis=1).astype(F32)
        at_ = [slice(n * cols + h * HEAD_DIM, n * cols + (h + 1) * HEAD_DIM) for n in range(4)]
        g = jnp.concatenate([gain[:, a] for a in at_], axis=1)
        w = jnp.concatenate([wo[a] for a in at_], axis=0)
        term = jnp.dot((x * g).astype(BF16), w, preferred_element_type=F32)
        return term, jnp.sum(x * x, axis=1, keepdims=True)

    def partial(h, k):
        rest(h, k)
        acc[k], sq[k] = share(h, k)

    def finish(h, k):
        rest(h, k)
        term, square = share(h, k)
        square = square + sq[k]
        out[seq(k)] = (
            (acc[k] + term) * lax.rsqrt(square / wo.shape[0] + NORM_FLOOR)
        ).astype(BF16)

    forward(0)
    ready(0)
    attend_close(0, 0)
    attend_far(0, 0)
    attend_close(0, 1)
    attend_far(0, 1)
    forward(1)
    for k in (0, 2):
        collect(0, k)
    for k in (0, 2):
        relay(0, k)
    for k in (1, 3):
        collect(0, k)
    for k in (1, 3):
        relay(0, k)
    ready(1)
    attend_close(1, 0)
    attend_far(1, 0)
    attend_close(1, 1)
    for k in (0, 2):
        collect(1, k)
    attend_far(1, 1)
    for k in (0, 2):
        relay(1, k)
    got_wo.wait()
    for k in (0, 2):
        partial(0, k)
    for k in (1, 3):
        collect(1, k)
    for k in (1, 3):
        partial(0, k)
    for k in (1, 3):
        relay(1, k)
    for k in (0, 2, 1, 3):
        finish(1, k)
    for k in range(seqs):
        for h in range(heads):
            w = l_copy(h, seq(k), lsend.at[0, :, :length], 0, (sp, right))
            if k == 0:
                unless(mine, w)
            else:
                w.wait_recv()
    for s in range(seqs):
        for h in range(heads):
            log_out[s, h : h + 1] = logs[s, h]
    for c_, there in sent:
        if there is None:
            c_.wait_send()
        else:

            @pl.when(there)
            def _(c_=c_):
                c_.wait_send()


def layer(nsp, ntp, tokens, wq, wk, wv, wo, tables, gain):
    seqs, length, width = tokens.shape
    cols = wq.shape[1]
    heads = cols // HEAD_DIM
    block = 2 * length
    wide = REACH * FAR
    own = seqs // 2 * block
    span = own + 2 * wide
    window = block + 2 * wide
    rows = block // FAR
    near_rows = rows + 2 * FAR
    per = FAR // NEAR
    grans = block // GRAN
    hbm = pl.BlockSpec(memory_space=pl.ANY)
    vmem = pl.BlockSpec(memory_space=pltpu.VMEM)
    v = pltpu.VMEM
    return pl.pallas_call(
        functools.partial(layer_kernel, nsp),
        in_specs=[hbm] * 7 + [vmem] * 3,
        out_specs=[vmem, vmem],
        out_shape=[
            jax.ShapeDtypeStruct((seqs, length, wo.shape[1]), BF16),
            jax.ShapeDtypeStruct((seqs, heads, length), F32),
        ],
        scratch_shapes=[
            v(tokens.shape, BF16), v(wq.shape, BF16), v(wk.shape, BF16), v(wv.shape, BF16),
            v(wo.shape, BF16), v((length, HEAD_DIM), F32), v((length, HEAD_DIM), F32),
            v((heads, span, 2 * HEAD_DIM), BF16),
            v((heads, own, HEAD_DIM), BF16),
            v((seqs * heads, length, 2 * HEAD_DIM), BF16),
            v((seqs * heads, length, HEAD_DIM), BF16),
            v((ntp, seqs, heads, length, HEAD_DIM), BF16),
            v((2 * heads, block, HEAD_DIM), BF16),
            v((seqs, heads, 1, length), F32),
            v((2 * heads, 1, block), F32),
            v((heads, FAR, span // FAR, 2 * HEAD_DIM), BF16),
            v((2, FAR, rows, HEAD_DIM), BF16),
            v((2, FAR, rows, HEAD_DIM), BF16),
            v((GRAN, GRAN), BF16),
            v((2, grans, GRAN, GRAN + 2 * REACH), F32),
            v((2, per * rows, per * near_rows), F32),
            v((2, rows, window // FAR), F32),
            v((2, FAR, rows, HEAD_DIM), F32),
            v((2, FAR, rows, HEAD_DIM), F32),
            v((2, FAR, rows, HEAD_DIM), F32),
            v((seqs, length, wo.shape[1]), F32),
            v((seqs, length, 1), F32),
            pltpu.SemaphoreType.DMA((seqs + 6,)),
            pltpu.SemaphoreType.DMA((68,)),
            pltpu.SemaphoreType.DMA((68,)),
        ],
        compiler_params=pltpu.CompilerParams(
            collective_id=0, has_side_effects=True, vmem_limit_bytes=56 * 2**20
        ),
        name="layer",
    )(tokens, wq, wk, wv, wo, *tables, gain)


def shards(tokens, query_weight, key_weight, value_weight, out_gain, out_weight):
    length = tokens.shape[1]
    nsp = lax.axis_size("sp")
    frequency = ROPE_BASE ** (-np.arange(HEAD_DIM // 2) / (HEAD_DIM // 2))
    frequency = np.tile(frequency, 2)[None, :]
    step = np.arange(length)[:, None] * frequency
    base = (np.arange(nsp) * length)[:, None] * frequency
    tables = [
        jnp.asarray(f(a).astype(np.float32)) for a in (step, base) for f in (np.cos, np.sin)
    ]
    return tuple(
        layer(
            nsp, lax.axis_size("tp"), tokens, query_weight, key_weight, value_weight,
            out_weight, tables, out_gain[None, :],
        )
    )


def solution(mesh):
    return jax.shard_map(
        shards,
        mesh=mesh,
        in_specs=(
            P(None, "sp", None),
            P(None, "tp"),
            P(None, "tp"),
            P(None, "tp"),
            P(),
            P(None, "tp"),
        ),
        out_specs=(P(None, "sp", "tp"), P(None, "tp", "sp")),
        check_vma=False,
    )
```

time: 82.4 us -> 82.6 us (level); the launches traced: 82.2 us -> 81.2 us
  Pallas kernels: 78.3 us -> 77.3 us
    pallas_call x1, Pallas kernels: 78.3 us -> 77.3 us  [layer(): pl.pallas_call(functools.partial(layer_kernel, nsp), in_specs=[hbm] * 7 +...]
where the time goes in v2:
time: 82.6 us; the launch traced here: 81.2 us
  Pallas kernels  77.3 us (94%)
  local copies, waits for them, and re-layouts  3.26 us (4%)
    pallas_call x1, Pallas kernels, layer(): pl.pallas_call(functools.partial(layer_kernel, nsp), in_specs=[hbm] * 7 +...  77.3 us
    unnamed x4, local copies, waits for them, and re-layouts  3.26 us

profile of v2, /device:TPU:160, one launch (start us, length us, event | category | flops | bytes accessed | tf_op | source)
XLA Modules:
  0.0 81.2 jit_solution(17196066753754067281)
XLA Ops:
  0.6 77.3 %layer.1 = (bf16[4,384,512]{2,1,0:T(8,128)(2,1)}, f32[4,2,384]{2,1,0:T(2,128)}) custom-call(bf16[4,384,2048]{2,1,0:T(8,128)(2,1)} %tok_h.1, bf16[2048,256]{1,0:T(8,128)(2,1)} %wq_h.1, bf16[2048,256]{1,0:T(8,128)(2,1)} %wk_h.1, bf16[2048,256]{1,0:T(8,128)(2,1)} %wv_h.1, bf16[1024,512]{1,0:T(8,128)(2,1)} %wo_h.1, f32[384,128]{1,0:T(8,128)} %constant.8.clone.cos_h, ...), custom_call_target="tpu_custom_call" | custom-call | tf_op jit(solution)/shard_map/layer/pallas_call | solution.py:578
  77.9 0.0 copy-start
  77.9 2.7 %copy.14 = bf16[4,384,512]{2,1,0:T(8,128)(2,1)} copy(bf16[4,384,512]{2,1,0:T(8,128)(2,1)} %get-tuple-element.4) | data formatting | bytes 3145728
  80.6 0.0 copy-done
  80.6 0.6 copy.15
Async XLA Ops:
  77.9 2.7 %copy-start = (f32[4,2,384]{2,1,0:T(2,128)S(1)}, f32[4,2,384]{2,1,0:T(2,128)}, u32[]{:S(2)}) copy-start(f32[4,2,384]{2,1,0:T(2,128)} %get-tuple-element.5) | copy-start | bytes 36868

commit v3 on v2

--- a/solution.py
+++ b/solution.py
@@ -43,7 +43,7 @@
 def layer_kernel(
     nsp, tok_h, wq_h, wk_h, wv_h, wo_h, cos_h, sin_h, cos_base, sin_base, gain,
     out, log_out,
-    tok, wq, wk, wv, wo, cos, sin, kn, qn, kvs, qs, gath, outs, logs, lsend,
+    tok, wq, wkv, wo, cos, sin, kn, qn, kvs, qs, gath, outs, logs, lsend,
     kp, qp, mp, perm, bias1, bias4, bias16, o1, m1, l1, acc, sq,
     load_sem, send_sem, recv_sem,
 ):
@@ -60,6 +60,8 @@
     near_rows = rows + 2 * FAR
     cols = wq.shape[1]
     heads = cols // HEAD_DIM
+    ends = wide // GRAN
+    stop = ends + own // GRAN
     total = nsp * length
     scale = HEAD_DIM**-0.5 * LOG2E
     sp, t = lax.axis_index("sp"), lax.axis_index("tp")
@@ -90,12 +92,25 @@
         loads.append(copy)
         return copy
 
-    order = (1, 3, 2, 0)
-    got_cos, got_sin = load(cos_h, cos), load(sin_h, sin)
-    got_wk, got_wv = load(wk_h, wk), load(wv_h, wv)
-    got_tok = {}
-    for k in order[:1]:
-        got_tok[k] = load(tok_h.at[seq(k)], tok.at[k])
+    def lanes(n):
+        return slice(n * HEAD_DIM, (n + 1) * HEAD_DIM)
+
+    def load_kv(h):
+        return (
+            load(wk_h.at[:, lanes(h)], wkv.at[h, :, lanes(0)]),
+            load(wv_h.at[:, lanes(h)], wkv.at[h, :, lanes(1)]),
+        )
+
+    def load_tok(k):
+        return load(tok_h.at[seq(k)], tok.at[k])
+
+    pairs = ((2, 0), (1, 3))
+    got_rope = (load(cos_h, cos), load(sin_h, sin))
+    got_first = (*load_kv(0), *[load_tok(k) for k in pairs[0]])
+    got_second = [load_tok(k) for k in pairs[1]]
+    got_wq = load(wq_h, wq)
+    got_third = load_kv(1)
+    got_wo = load(wo_h, wo)
 
     barrier = pltpu.get_barrier_semaphore()
 
@@ -222,73 +237,84 @@
             22 + 3 * h + p, 22 + 3 * h + p, half_at(part - 1),
         )
 
-    def forward(h):
-        for j in range(4):
-            unless(is_here(j), kv_copy(h, 0, j))
-            if j < 3:
-                start(down(h, j), below)
-            if j > 0:
-                start(up(h, j - 1), above)
+    flip = y % 2 == 1
+
+    def forward(h, far):
+        def relay_in(js):
+            for j in js:
+                unless(is_here(j), kv_copy(h, 0, j))
+                if j < 3:
+
+                    @pl.when(below)
+                    def _(j=j):
+                        down(h, j).start()
+
+                if j > 0:
+
+                    @pl.when(above)
+                    def _(j=j):
+                        up(h, j - 1).start()
+
+        @pl.when(flip != far)
+        def _():
+            relay_in((2, 3))
+
+        @pl.when(flip == far)
+        def _():
+            relay_in((0, 1))
+
+        if far:
+            for p in range(3):
+                sent.append((down(h, p), below))
+                sent.append((up(h, p), above))
 
     def halo(h):
         for p in range(3):
             unless(jnp.logical_not(below), up(h, p))
             unless(jnp.logical_not(above), down(h, p))
 
-    def lanes(n):
-        return slice(n * HEAD_DIM, (n + 1) * HEAD_DIM)
-
-    def turned(x, w, store):
-        a = jnp.dot(x, w[...], preferred_element_type=F32)
-        for h in range(heads):
-            one = a[:, lanes(h)]
-            store(h, (one * cos[...] + pltpu.roll(one, HEAD_DIM // 2, 1) * sin[...]).astype(BF16))
-
-    def project_kv(k):
-        x = tok[k]
-
-        def put(h, a):
-            kvs[k * heads + h, :, :HEAD_DIM] = a
-
-        turned(x, wk, put)
-        v = jnp.dot(x, wv[...], preferred_element_type=F32).astype(BF16)
-        for h in range(heads):
-            kvs[k * heads + h, :, HEAD_DIM:] = v[:, lanes(h)]
-
-    def project_q(k):
-        def put(h, a):
-            qs[k * heads + h] = a
-
-        turned(tok[k], wq, put)
+    def turned(one):
+        return (one * cos[...] + pltpu.roll(one, HEAD_DIM // 2, 1) * sin[...]).astype(BF16)
+
+    def project_kv(h, ks):
+        both = [jnp.dot(tok[k], wkv[h], preferred_element_type=F32) for k in ks]
+        for k, a in zip(ks, both):
+            kvs[k * heads + h, :, lanes(0)] = turned(a[:, lanes(0)])
+            kvs[k * heads + h, :, lanes(1)] = a[:, lanes(1)].astype(BF16)
+
+    def project_q(ks):
+        both = [jnp.dot(tok[k], wq[...], preferred_element_type=F32) for k in ks]
+        for k, a in zip(ks, both):
+            for h in range(heads):
+                qs[k * heads + h] = turned(a[:, lanes(h)])
 
     cos_at, sin_at = cos_base[pl.ds(sp, 1)], sin_base[pl.ds(sp, 1)]
     sign = jnp.where(iota(cos.shape, 1) < HEAD_DIM // 2, -1.0, 1.0)
-    got_cos.wait()
-    got_sin.wait()
+    for c_ in got_rope:
+        c_.wait()
     cos_step, sin_step = cos[...], sin[...]
     cos[...] = cos_step * cos_at - sin_step * sin_at
     sin[...] = (sin_step * cos_at + cos_step * sin_at) * sign
-    for c_ in (got_wk, got_wv, got_tok[order[0]]):
+    for c_ in got_first:
         c_.wait()
-    for k in order[1:]:
-        got_tok[k] = load(tok_h.at[seq(k)], tok.at[k])
-    got_wq = load(wq_h, wq)
-    got_wo = load(wo_h, wo)
-    project_kv(order[0])
+    project_kv(0, pairs[0])
     pl.semaphore_wait(barrier, count)
-    kv_send(0, order[0])
-    for k in order[1:]:
-        got_tok[k].wait()
-        project_kv(k)
+    for k in pairs[0]:
+        kv_send(0, k)
+    for c_ in got_second:
+        c_.wait()
+    project_kv(0, pairs[1])
+    for k in pairs[1]:
         kv_send(0, k)
     got_wq.wait()
-    for k in order:
-        project_q(k)
-        q_send(0, k)
-    for k in order:
-        kv_send(1, k)
-    for k in order:
-        q_send(1, k)
+    for ks in pairs:
+        project_q(ks)
+        for k in ks:
+            q_send(0, k)
+    for c_ in got_third:
+        c_.wait()
+    for ks in pairs:
+        project_kv(1, ks)
 
     perm[...] = jnp.where(
         iota((GRAN, GRAN), 1) == perm_token(iota((GRAN, GRAN), 0)), 1.0, 0.0
@@ -327,39 +353,43 @@
             moved = moved.astype(BF16).reshape(FAR, FAR, 2 * HEAD_DIM)
             kp[h, :, j * FAR : (j + 1) * FAR] = moved
 
-    def ready(h):
-        gather_keys(h, range(side, (wide + own) // GRAN))
-        for j in range(4):
+    def gather_own(h):
+        gather_keys(h, range(ends, stop))
+
+    def gather_ends(h):
+        gather_keys(h, [*range(ends), *range(stop, span // GRAN)])
+
+    def queries(h, step):
+        for i in range(2):
+            j = (step + y) % 2 * 2 + i
             unless(is_here(j), q_copy(h, 0, j))
-        halo(h)
-        gather_keys(h, [*range(side), *range((wide + own) // GRAN, span // GRAN)])
-
-    def attend_close(h, step):
-        slot = step
+
+    def close(h, step, g):
         jb = (step + y) % 2
-        off = jb * block
-        for g in range(grans):
-            moved = jnp.dot(
-                perm[...],
-                qn[h, pl.ds(pl.multiple_of(off + g * GRAN, GRAN), GRAN)],
-                preferred_element_type=F32,
-            )
-            moved = moved.astype(BF16)
-            qp[slot, :, g * FAR : (g + 1) * FAR] = moved.reshape(FAR, FAR, HEAD_DIM)
-            near = pl.ds(
-                pl.multiple_of(off + wide + g * GRAN - REACH, REACH), GRAN + 2 * REACH
-            )
-            k = kn[h, near, :HEAD_DIM]
-            v = kn[h, near, HEAD_DIM:]
-            sc = dot_t(moved, k) * scale + bias1[jb, g]
-            m = jnp.max(sc, axis=1, keepdims=True)
-            p = jnp.exp2(sc - m)
-            l = jnp.sum(p, axis=1, keepdims=True)
-            o = jnp.dot(p.astype(BF16), v, preferred_element_type=F32)
-            cut = (FAR, FAR, HEAD_DIM)
-            o1[slot, :, g * FAR : (g + 1) * FAR] = o.reshape(cut)
-            m1[slot, :, g * FAR : (g + 1) * FAR] = jnp.broadcast_to(m, o.shape).reshape(cut)
-            l1[slot, :, g * FAR : (g + 1) * FAR] = jnp.broadcast_to(l, o.shape).reshape(cut)
+        q_at = pl.multiple_of(jb * block + g * GRAN, GRAN)
+        near = pl.ds(pl.multiple_of(q_at + wide - REACH, REACH), GRAN + 2 * REACH)
+        sl = pl.ds(pl.multiple_of(g * FAR, FAR), FAR)
+        moved = jnp.dot(perm[...], qn[h, pl.ds(q_at, GRAN)], preferred_element_type=F32)
+        moved = moved.astype(BF16)
+        qp[step, :, sl] = moved.reshape(FAR, FAR, HEAD_DIM)
+        k = kn[h, near, lanes(0)]
+        v = kn[h, near, lanes(1)]
+        sc = dot_t(moved, k) * scale + bias1[jb, g]
+        m = jnp.max(sc, axis=1, keepdims=True)
+        p = jnp.exp2(sc - m)
+        l = jnp.sum(p, axis=1, keepdims=True)
+        o = jnp.dot(p.astype(BF16), v, preferred_element_type=F32)
+        cut = (FAR, FAR, HEAD_DIM)
+        o1[step, :, sl] = o.reshape(cut)
+        m1[step, :, sl] = jnp.broadcast_to(m, o.shape).reshape(cut)
+        l1[step, :, sl] = jnp.broadcast_to(l, o.shape).reshape(cut)
+
+    def close_inner(h, step):
+        for i in range(1, grans):
+            close(h, step, i - (step + y) % 2)
+
+    def close_outer(h, step):
+        close(h, step, (step + y) % 2 * (grans - 1))
 
     def attend_far(h, step):
         slot = step
@@ -458,14 +488,30 @@
         n = 44 + 8 * kind + 2 * k + h
         return copy(ref, ref, n, n, (sp, to))
 
-    def collect(h, k):
-        w = o_copy(h, seq(k), outs.at[0, :length], 0, (sp, right))
-        if k == 0:
-            unless(mine, w)
-        else:
-            w.wait_recv()
-        start(piece(0, h, k, t, right))
-        start(piece(1, h, k, t, left))
+    def collect(h, *ks):
+        for k in ks:
+            o_copy(h, seq(k), outs.at[0, :length], 0, (sp, right)).wait_recv()
+        for a, b in zip(ks, reversed(ks)):
+            start(piece(0, h, a, t, right))
+            start(piece(1, h, b, t, left))
+
+    def spread(h):
+        piece(0, h, 0, t, right).start()
+        piece(1, h, 0, t, left).start()
+
+    def collect_mine(h):
+        @pl.when(mine)
+        def _():
+            spread(h)
+
+    def collect_twin(h):
+        @pl.when(jnp.logical_not(mine))
+        def _():
+            o_copy(h, y, outs.at[0, :length], 0, (sp, right)).wait_recv()
+            spread(h)
+
+        sent.append((piece(0, h, 0, t, right), None))
+        sent.append((piece(1, h, 0, t, left), None))
 
     def relay(h, k):
         if k in (0, 1):
@@ -504,39 +550,61 @@
             (acc[k] + term) * lax.rsqrt(square / wo.shape[0] + NORM_FLOOR)
         ).astype(BF16)
 
-    forward(0)
-    ready(0)
-    attend_close(0, 0)
+    forward(0, False)
+    forward(0, True)
+    for k in pairs[0]:
+        kv_send(1, k)
+    for k in pairs[0]:
+        q_send(1, k)
+    for k in pairs[1]:
+        kv_send(1, k)
+    gather_own(0)
+    queries(0, 0)
+    close_inner(0, 0)
+    halo(0)
+    gather_ends(0)
+    close_outer(0, 0)
     attend_far(0, 0)
-    attend_close(0, 1)
+    for k in pairs[1]:
+        q_send(1, k)
+    collect_mine(0)
+    forward(1, False)
+    queries(0, 1)
+    close_inner(0, 1)
+    close_outer(0, 1)
     attend_far(0, 1)
-    forward(1)
-    for k in (0, 2):
-        collect(0, k)
-    for k in (0, 2):
-        relay(0, k)
-    for k in (1, 3):
-        collect(0, k)
-    for k in (1, 3):
-        relay(0, k)
-    ready(1)
-    attend_close(1, 0)
+    collect_twin(0)
+    forward(1, True)
+    gather_own(1)
+    queries(1, 0)
+    close_inner(1, 0)
+    collect(0, 2)
+    relay(0, 0)
+    halo(1)
+    gather_ends(1)
+    close_outer(1, 0)
+    collect(0, 1, 3)
     attend_far(1, 0)
-    attend_close(1, 1)
-    for k in (0, 2):
-        collect(1, k)
+    relay(0, 2)
+    collect_mine(1)
+    queries(1, 1)
+    close_inner(1, 1)
+    close_outer(1, 1)
+    relay(0, 1)
     attend_far(1, 1)
-    for k in (0, 2):
-        relay(1, k)
+    relay(0, 3)
+    collect_twin(1)
+    collect(1, 2)
     got_wo.wait()
-    for k in (0, 2):
-        partial(0, k)
-    for k in (1, 3):
-        collect(1, k)
-    for k in (1, 3):
-        partial(0, k)
-    for k in (1, 3):
-        relay(1, k)
+    partial(0, 0)
+    relay(1, 0)
+    partial(0, 2)
+    collect(1, 1, 3)
+    relay(1, 2)
+    partial(0, 1)
+    partial(0, 3)
+    relay(1, 1)
+    relay(1, 3)
     for k in (0, 2, 1, 3):
         finish(1, k)
     for k in range(seqs):
@@ -580,11 +648,11 @@
         in_specs=[hbm] * 7 + [vmem] * 3,
         out_specs=[vmem, vmem],
         out_shape=[
-            jax.ShapeDtypeStruct((seqs, length, wo.shape[1]), BF16),
-            jax.ShapeDtypeStruct((seqs, heads, length), F32),
+            v((seqs, length, wo.shape[1]), BF16),
+            v((seqs, heads, length), F32),
         ],
         scratch_shapes=[
-            v(tokens.shape, BF16), v(wq.shape, BF16), v(wk.shape, BF16), v(wv.shape, BF16),
+            v(tokens.shape, BF16), v(wq.shape, BF16), v((heads, width, 2 * HEAD_DIM), BF16),
             v(wo.shape, BF16), v((length, HEAD_DIM), F32), v((length, HEAD_DIM), F32),
             v((heads, span, 2 * HEAD_DIM), BF16),
             v((heads, own, HEAD_DIM), BF16),
@@ -606,7 +674,7 @@
             v((2, FAR, rows, HEAD_DIM), F32),
             v((seqs, length, wo.shape[1]), F32),
             v((seqs, length, 1), F32),
-            pltpu.SemaphoreType.DMA((seqs + 6,)),
+            pltpu.SemaphoreType.DMA((seqs + 8,)),
             pltpu.SemaphoreType.DMA((68,)),
             pltpu.SemaphoreType.DMA((68,)),
         ],
@@ -615,6 +683,32 @@
         ),
         name="layer",
     )(tokens, wq, wk, wv, wo, *tables, gain)
+
+
+def store_kernel(mixed, logs, mixed_out, log_out, sem):
+    copies = [
+        pltpu.make_async_copy(mixed.at[s], mixed_out.at[s], sem.at[s])
+        for s in range(mixed.shape[0])
+    ]
+    copies.append(pltpu.make_async_copy(logs, log_out, sem.at[mixed.shape[0]]))
+    for c in copies:
+        c.start()
+    for c in copies:
+        c.wait()
+
+
+def store(mixed, logs):
+    hbm = pl.BlockSpec(memory_space=pl.ANY)
+    vmem = pl.BlockSpec(memory_space=pltpu.VMEM)
+    return pl.pallas_call(
+        store_kernel,
+        in_specs=[vmem] * 2,
+        out_specs=[hbm] * 2,
+        out_shape=[jax.ShapeDtypeStruct(a.shape, a.dtype) for a in (mixed, logs)],
+        scratch_shapes=[pltpu.SemaphoreType.DMA((mixed.shape[0] + 1,))],
+        compiler_params=pltpu.CompilerParams(vmem_limit_bytes=2**20),
+        name="store",
+    )(mixed, logs)
 
 
 def shards(tokens, query_weight, key_weight, value_weight, out_gain, out_weight):
@@ -628,10 +722,10 @@
         jnp.asarray(f(a).astype(np.float32)) for a in (step, base) for f in (np.cos, np.sin)
     ]
     return tuple(
-        layer(
+        store(*layer(
             nsp, lax.axis_size("tp"), tokens, query_weight, key_weight, value_weight,
             out_weight, tables, out_gain[None, :],
-        )
+        ))
     )
 
 

time: 82.6 us -> 67.1 us (0.81)
  the two profiles are of different devices: /device:TPU:160 before, /device:TPU:199 now
where the time goes in v3:
time: 67.1 us; the launch traced here: 67 us
  Pallas kernels  66.1 us (99%)
  between operations  0.82 us (1%)
    pallas_call x1, Pallas kernels, layer(): pl.pallas_call(functools.partial(layer_kernel, nsp), in_specs=[hbm] * 7 +...  65 us

profile of v3, /device:TPU:199, one launch (start us, length us, event | category | flops | bytes accessed | tf_op | source)
XLA Modules:
  0.0 67.0 jit_solution(522838150568856247)
XLA Ops:
  0.6 65.0 %layer.1 = (bf16[4,384,512]{2,1,0:T(8,128)(2,1)S(1)}, f32[4,2,384]{2,1,0:T(2,128)S(1)}) custom-call(bf16[4,384,2048]{2,1,0:T(8,128)(2,1)} %tok_h.1, bf16[2048,256]{1,0:T(8,128)(2,1)} %wq_h.1, bf16[2048,256]{1,0:T(8,128)(2,1)} %wk_h.1, bf16[2048,256]{1,0:T(8,128)(2,1)} %wv_h.1, bf16[1024,512]{1,0:T(8,128)(2,1)} %wo_h.1, f32[384,128]{1,0:T(8,128)} %constant.8.clone.cos_h, ...), custom_call_target="tpu_custom_call" | custom-call | tf_op jit(solution)/shard_map/layer/pallas_call | solution.py:646
  65.6 1.2 %store.1 = (bf16[4,384,512]{2,1,0:T(8,128)(2,1)}, f32[4,2,384]{2,1,0:T(2,128)}) custom-call(bf16[4,384,512]{2,1,0:T(8,128)(2,1)S(1)} %get-tuple-element.4.mixed, f32[4,2,384]{2,1,0:T(2,128)S(1)} %get-tuple-element.5.logs), custom_call_target="tpu_custom_call" | custom-call | tf_op jit(solution)/shard_map/store/pallas_call | solution.py:703

commit v4 on v3

--- a/solution.py
+++ b/solution.py
@@ -106,9 +106,9 @@
 
     pairs = ((2, 0), (1, 3))
     got_rope = (load(cos_h, cos), load(sin_h, sin))
-    got_first = (*load_kv(0), *[load_tok(k) for k in pairs[0]])
+    got_first = (*load_kv(0), load_tok(2))
     got_second = [load_tok(k) for k in pairs[1]]
-    got_wq = load(wq_h, wq)
+    got_wq = (load(wq_h, wq), load_tok(0))
     got_third = load_kv(1)
     got_wo = load(wo_h, wo)
 
@@ -276,11 +276,14 @@
     def turned(one):
         return (one * cos[...] + pltpu.roll(one, HEAD_DIM // 2, 1) * sin[...]).astype(BF16)
 
+    def store_kv(h, k, a):
+        kvs[k * heads + h, :, lanes(0)] = turned(a[:, lanes(0)])
+        kvs[k * heads + h, :, lanes(1)] = a[:, lanes(1)].astype(BF16)
+
     def project_kv(h, ks):
         both = [jnp.dot(tok[k], wkv[h], preferred_element_type=F32) for k in ks]
         for k, a in zip(ks, both):
-            kvs[k * heads + h, :, lanes(0)] = turned(a[:, lanes(0)])
-            kvs[k * heads + h, :, lanes(1)] = a[:, lanes(1)].astype(BF16)
+            store_kv(h, k, a)
 
     def project_q(ks):
         both = [jnp.dot(tok[k], wq[...], preferred_element_type=F32) for k in ks]
@@ -297,16 +300,27 @@
     sin[...] = (sin_step * cos_at + cos_step * sin_at) * sign
     for c_ in got_first:
         c_.wait()
-    project_kv(0, pairs[0])
+    cut = length // 2
+    halves = [
+        jnp.dot(tok[2, i * cut : (i + 1) * cut], wkv[0], preferred_element_type=F32)
+        for i in range(2)
+    ]
+    store_kv(0, 2, jnp.concatenate(halves, axis=0))
     pl.semaphore_wait(barrier, count)
-    for k in pairs[0]:
-        kv_send(0, k)
+    kv_send(0, 2)
     for c_ in got_second:
         c_.wait()
     project_kv(0, pairs[1])
     for k in pairs[1]:
         kv_send(0, k)
-    got_wq.wait()
+    for c_ in got_wq:
+        c_.wait()
+    halves = [
+        jnp.dot(tok[0, i * cut : (i + 1) * cut], wkv[0], preferred_element_type=F32)
+        for i in range(2)
+    ]
+    store_kv(0, 0, jnp.concatenate(halves, axis=0))
+    kv_send(0, 0)
     for ks in pairs:
         project_q(ks)
         for k in ks:
@@ -391,7 +405,7 @@
     def close_outer(h, step):
         close(h, step, (step + y) % 2 * (grans - 1))
 
-    def attend_far(h, step):
+    def attend_far(h, step, between=None):
         slot = step
         hs = 2 * h + step
         jb = (step + y) % 2
@@ -439,6 +453,8 @@
             )
             o = o1[slot, sel].reshape(flat) * keep + o16
             o = o + jnp.dot(p4.astype(BF16), v4, preferred_element_type=F32)
+            if between is not None and group == NEAR // 2:
+                between()
             mp[slot, sel] = (o / l).astype(BF16).reshape(per, rows, HEAD_DIM)
             m1[slot, sel] = (m_new * LN2 + jnp.log(l)).reshape(per, rows, HEAD_DIM)
         lane = iota((GRAN, HEAD_DIM), 1)
@@ -552,12 +568,11 @@
 
     forward(0, False)
     forward(0, True)
-    for k in pairs[0]:
-        kv_send(1, k)
+    for ks in pairs:
+        for k in ks:
+            kv_send(1, k)
     for k in pairs[0]:
         q_send(1, k)
-    for k in pairs[1]:
-        kv_send(1, k)
     gather_own(0)
     queries(0, 0)
     close_inner(0, 0)
@@ -565,16 +580,19 @@
     gather_ends(0)
     close_outer(0, 0)
     attend_far(0, 0)
-    for k in pairs[1]:
-        q_send(1, k)
     collect_mine(0)
     forward(1, False)
     queries(0, 1)
     close_inner(0, 1)
     close_outer(0, 1)
-    attend_far(0, 1)
-    collect_twin(0)
-    forward(1, True)
+
+    def half_way():
+        collect_twin(0)
+        forward(1, True)
+
+    attend_far(0, 1, half_way)
+    for k in pairs[1]:
+        q_send(1, k)
     gather_own(1)
     queries(1, 0)
     close_inner(1, 0)
@@ -590,23 +608,31 @@
     queries(1, 1)
     close_inner(1, 1)
     close_outer(1, 1)
+    collect_twin(1)
     relay(0, 1)
-    attend_far(1, 1)
+    attend_far(1, 1, lambda: collect(1, 2))
     relay(0, 3)
-    collect_twin(1)
-    collect(1, 2)
     got_wo.wait()
     partial(0, 0)
     relay(1, 0)
     partial(0, 2)
+    relay(1, 2)
+    done = len(sent)
     collect(1, 1, 3)
-    relay(1, 2)
     partial(0, 1)
     partial(0, 3)
-    relay(1, 1)
-    relay(1, 3)
-    for k in (0, 2, 1, 3):
-        finish(1, k)
+
+    def settle(some):
+        for c_, there in some:
+            if there is None:
+                c_.wait_send()
+            else:
+
+                @pl.when(there)
+                def _(c_=c_):
+                    c_.wait_send()
+
+    settle(sent[:done])
     for k in range(seqs):
         for h in range(heads):
             w = l_copy(h, seq(k), lsend.at[0, :, :length], 0, (sp, right))
@@ -617,14 +643,11 @@
     for s in range(seqs):
         for h in range(heads):
             log_out[s, h : h + 1] = logs[s, h]
-    for c_, there in sent:
-        if there is None:
-            c_.wait_send()
-        else:
-
-            @pl.when(there)
-            def _(c_=c_):
-                c_.wait_send()
+    relay(1, 1)
+    relay(1, 3)
+    for k in (0, 2, 1, 3):
+        finish(1, k)
+    settle(sent[done:])
 
 
 def layer(nsp, ntp, tokens, wq, wk, wv, wo, tables, gain):

time: 67.1 us -> 64.4 us (0.960)
  the two profiles are of different devices: /device:TPU:199 before, /device:TPU:160 now
where the time goes in v4:
time: 64.4 us; the launch traced here: 63.8 us
  Pallas kernels  63 us (98%)
  between operations  0.82 us (1%)
    pallas_call x1, Pallas kernels, layer(): pl.pallas_call(functools.partial(layer_kernel, nsp), in_specs=[hbm] * 7 +...  61.8 us

profile of v4, /device:TPU:160, one launch (start us, length us, event | category | flops | bytes accessed | tf_op | source)
XLA Modules:
  0.0 63.8 jit_solution(16432918409196059764)
XLA Ops:
  0.6 61.8 %layer.1 = (bf16[4,384,512]{2,1,0:T(8,128)(2,1)S(1)}, f32[4,2,384]{2,1,0:T(2,128)S(1)}) custom-call(bf16[4,384,2048]{2,1,0:T(8,128)(2,1)} %tok_h.1, bf16[2048,256]{1,0:T(8,128)(2,1)} %wq_h.1, bf16[2048,256]{1,0:T(8,128)(2,1)} %wk_h.1, bf16[2048,256]{1,0:T(8,128)(2,1)} %wv_h.1, bf16[1024,512]{1,0:T(8,128)(2,1)} %wo_h.1, f32[384,128]{1,0:T(8,128)} %constant.8.clone.cos_h, ...), custom_call_target="tpu_custom_call" | custom-call | tf_op jit(solution)/shard_map/layer/pallas_call | solution.py:669
  62.4 1.2 %store.1 = (bf16[4,384,512]{2,1,0:T(8,128)(2,1)}, f32[4,2,384]{2,1,0:T(2,128)}) custom-call(bf16[4,384,512]{2,1,0:T(8,128)(2,1)S(1)} %get-tuple-element.4.mixed, f32[4,2,384]{2,1,0:T(2,128)S(1)} %get-tuple-element.5.logs), custom_call_target="tpu_custom_call" | custom-call | tf_op jit(solution)/shard_map/store/pallas_call | solution.py:726

commit v5 on v4

--- a/solution.py
+++ b/solution.py
@@ -330,6 +330,7 @@
     for ks in pairs:
         project_kv(1, ks)
 
+    forward(0, False)
     perm[...] = jnp.where(
         iota((GRAN, GRAN), 1) == perm_token(iota((GRAN, GRAN), 0)), 1.0, 0.0
     ).astype(BF16)
@@ -566,13 +567,10 @@
             (acc[k] + term) * lax.rsqrt(square / wo.shape[0] + NORM_FLOOR)
         ).astype(BF16)
 
-    forward(0, False)
     forward(0, True)
     for ks in pairs:
         for k in ks:
             kv_send(1, k)
-    for k in pairs[0]:
-        q_send(1, k)
     gather_own(0)
     queries(0, 0)
     close_inner(0, 0)
@@ -581,6 +579,8 @@
     close_outer(0, 0)
     attend_far(0, 0)
     collect_mine(0)
+    for k in pairs[0]:
+        q_send(1, k)
     forward(1, False)
     queries(0, 1)
     close_inner(0, 1)
@@ -594,10 +594,10 @@
     for k in pairs[1]:
         q_send(1, k)
     gather_own(1)
+    collect(0, 2)
+    relay(0, 0)
     queries(1, 0)
     close_inner(1, 0)
-    collect(0, 2)
-    relay(0, 0)
     halo(1)
     gather_ends(1)
     close_outer(1, 0)

time: 64.4 us -> 64.1 us (level)
  no operation moved by 1% of the time
where the time goes in v5:
time: 64.1 us; the launch traced here: 64 us
  Pallas kernels  63.2 us (99%)
  between operations  0.82 us (1%)
    pallas_call x1, Pallas kernels, layer(): pl.pallas_call(functools.partial(layer_kernel, nsp), in_specs=[hbm] * 7 +...  62 us

profile of v5, /device:TPU:160, one launch (start us, length us, event | category | flops | bytes accessed | tf_op | source)
XLA Modules:
  0.0 64.0 jit_solution(4287986780996144485)
XLA Ops:
  0.6 62.0 %layer.1 = (bf16[4,384,512]{2,1,0:T(8,128)(2,1)S(1)}, f32[4,2,384]{2,1,0:T(2,128)S(1)}) custom-call(bf16[4,384,2048]{2,1,0:T(8,128)(2,1)} %tok_h.1, bf16[2048,256]{1,0:T(8,128)(2,1)} %wq_h.1, bf16[2048,256]{1,0:T(8,128)(2,1)} %wk_h.1, bf16[2048,256]{1,0:T(8,128)(2,1)} %wv_h.1, bf16[1024,512]{1,0:T(8,128)(2,1)} %wo_h.1, f32[384,128]{1,0:T(8,128)} %constant.8.clone.cos_h, ...), custom_call_target="tpu_custom_call" | custom-call | tf_op jit(solution)/shard_map/layer/pallas_call | solution.py:669
  62.6 1.2 %store.1 = (bf16[4,384,512]{2,1,0:T(8,128)(2,1)}, f32[4,2,384]{2,1,0:T(2,128)}) custom-call(bf16[4,384,512]{2,1,0:T(8,128)(2,1)S(1)} %get-tuple-element.4.mixed, f32[4,2,384]{2,1,0:T(2,128)S(1)} %get-tuple-element.5.logs), custom_call_target="tpu_custom_call" | custom-call | tf_op jit(solution)/shard_map/store/pallas_call | solution.py:726

commit v6 on v5

--- a/solution.py
+++ b/solution.py
@@ -186,9 +186,13 @@
     def q_chunk(j):
         return pl.ds(pl.multiple_of(j * length, HEAD_DIM), length)
 
-    def kv_copy(h, k, j):
+    piece_rows = length // 2
+
+    def kv_copy(h, k, j, i):
+        at_ = pl.ds(pl.multiple_of(wide + j * length + i * piece_rows, REACH), piece_rows)
+        n = 68 * i + h * 4
         return copy(
-            kvs.at[k * heads + h], kn.at[h, chunk(j)], h * 4 + k, h * 4 + j,
+            kvs.at[k * heads + h, pl.ds(i * piece_rows, piece_rows)], kn.at[h, at_], n + k, n + j,
             at(z, seq(k), worker),
         )
 
@@ -208,7 +212,8 @@
             def _():
                 kn[h, chunk(place)] = kvs[h]
 
-        start(kv_copy(h, k, place), jnp.logical_not(mine) if k == 0 else None)
+        for i in range(2):
+            start(kv_copy(h, k, place, i), jnp.logical_not(mine) if k == 0 else None)
 
     def q_send(h, k):
         if k == 0:
@@ -219,41 +224,42 @@
 
         start(q_copy(h, k, place), jnp.logical_not(mine) if k == 0 else None)
 
-    first_up = wide + own - wide
-    cuts_up = [(first_up, 2 * length - (own - wide)), (wide + 2 * length, length), (wide + 3 * length, length)]
-    cuts_down = [(wide, length), (wide + length, length), (wide + 2 * length, wide - 2 * length)]
+    spans = [(max(n * piece_rows, own - wide), (n + 1) * piece_rows) for n in range(8)]
+    cuts_up = [(wide + a, b - a) for a, b in spans if b > a]
+    spans = [(n * piece_rows, min((n + 1) * piece_rows, wide)) for n in range(8)]
+    cuts_down = [(wide + a, b - a) for a, b in spans if b > a]
 
     def up(h, p):
         row, size = cuts_up[p]
         return copy(
             kn.at[h, row : row + size], kn.at[h, row - own : row - own + size],
-            16 + 3 * h + p, 16 + 3 * h + p, half_at(part + 1),
+            76 + 6 * h + p, 76 + 6 * h + p, half_at(part + 1),
         )
 
     def down(h, p):
         row, size = cuts_down[p]
         return copy(
             kn.at[h, row : row + size], kn.at[h, row + own : row + own + size],
-            22 + 3 * h + p, 22 + 3 * h + p, half_at(part - 1),
+            88 + 6 * h + p, 88 + 6 * h + p, half_at(part - 1),
         )
 
     flip = y % 2 == 1
 
     def forward(h, far):
         def relay_in(js):
-            for j in js:
-                unless(is_here(j), kv_copy(h, 0, j))
-                if j < 3:
+            for n in [2 * j + i for j in js for i in range(2)]:
+                unless(is_here(n // 2), kv_copy(h, 0, n // 2, n % 2))
+                if n < 6:
 
                     @pl.when(below)
-                    def _(j=j):
-                        down(h, j).start()
-
-                if j > 0:
+                    def _(n=n):
+                        down(h, n).start()
+
+                if n > 1:
 
                     @pl.when(above)
-                    def _(j=j):
-                        up(h, j - 1).start()
+                    def _(n=n):
+                        up(h, n - 2).start()
 
         @pl.when(flip != far)
         def _():
@@ -264,12 +270,12 @@
             relay_in((0, 1))
 
         if far:
-            for p in range(3):
+            for p in range(6):
                 sent.append((down(h, p), below))
                 sent.append((up(h, p), above))
 
     def halo(h):
-        for p in range(3):
+        for p in range(6):
             unless(jnp.logical_not(below), up(h, p))
             unless(jnp.logical_not(above), down(h, p))
 
@@ -609,16 +615,16 @@
     close_inner(1, 1)
     close_outer(1, 1)
     collect_twin(1)
-    relay(0, 1)
-    attend_far(1, 1, lambda: collect(1, 2))
+    attend_far(1, 1, lambda: relay(0, 1))
+    collect(1, 2)
     relay(0, 3)
+    relay(1, 0)
     got_wo.wait()
     partial(0, 0)
-    relay(1, 0)
     partial(0, 2)
-    relay(1, 2)
     done = len(sent)
     collect(1, 1, 3)
+    relay(1, 2)
     partial(0, 1)
     partial(0, 3)
 
@@ -698,8 +704,8 @@
             v((seqs, length, wo.shape[1]), F32),
             v((seqs, length, 1), F32),
             pltpu.SemaphoreType.DMA((seqs + 8,)),
-            pltpu.SemaphoreType.DMA((68,)),
-            pltpu.SemaphoreType.DMA((68,)),
+            pltpu.SemaphoreType.DMA((100,)),
+            pltpu.SemaphoreType.DMA((100,)),
         ],
         compiler_params=pltpu.CompilerParams(
             collective_id=0, has_side_effects=True, vmem_limit_bytes=56 * 2**20

time: 64.1 us -> 64 us (level)
  no operation moved by 1% of the time
where the time goes in v6:
time: 64 us; the launch traced here: 63.5 us
  Pallas kernels  62.6 us (98%)
  between operations  0.82 us (1%)
    pallas_call x1, Pallas kernels, layer(): pl.pallas_call(functools.partial(layer_kernel, nsp), in_specs=[hbm] * 7 +...  61.5 us

profile of v6, /device:TPU:160, one launch (start us, length us, event | category | flops | bytes accessed | tf_op | source)
XLA Modules:
  0.0 63.5 jit_solution(14714460330738117301)
XLA Ops:
  0.6 61.5 %layer.1 = (bf16[4,384,512]{2,1,0:T(8,128)(2,1)S(1)}, f32[4,2,384]{2,1,0:T(2,128)S(1)}) custom-call(bf16[4,384,2048]{2,1,0:T(8,128)(2,1)} %tok_h.1, bf16[2048,256]{1,0:T(8,128)(2,1)} %wq_h.1, bf16[2048,256]{1,0:T(8,128)(2,1)} %wk_h.1, bf16[2048,256]{1,0:T(8,128)(2,1)} %wv_h.1, bf16[1024,512]{1,0:T(8,128)(2,1)} %wo_h.1, f32[384,128]{1,0:T(8,128)} %constant.8.clone.cos_h, ...), custom_call_target="tpu_custom_call" | custom-call | tf_op jit(solution)/shard_map/layer/pallas_call | solution.py:675
  62.1 1.2 %store.1 = (bf16[4,384,512]{2,1,0:T(8,128)(2,1)}, f32[4,2,384]{2,1,0:T(2,128)}) custom-call(bf16[4,384,512]{2,1,0:T(8,128)(2,1)S(1)} %get-tuple-element.4.mixed, f32[4,2,384]{2,1,0:T(2,128)S(1)} %get-tuple-element.5.logs), custom_call_target="tpu_custom_call" | custom-call | tf_op jit(solution)/shard_map/store/pallas_call | solution.py:732

commit v7 on v6

--- a/solution.py
+++ b/solution.py
@@ -279,8 +279,9 @@
             unless(jnp.logical_not(below), up(h, p))
             unless(jnp.logical_not(above), down(h, p))
 
-    def turned(one):
-        return (one * cos[...] + pltpu.roll(one, HEAD_DIM // 2, 1) * sin[...]).astype(BF16)
+    def turned(one, by=None):
+        a = one * cos[...] + pltpu.roll(one, HEAD_DIM // 2, 1) * sin[...]
+        return (a if by is None else a * by).astype(BF16)
 
     def store_kv(h, k, a):
         kvs[k * heads + h, :, lanes(0)] = turned(a[:, lanes(0)])
@@ -295,7 +296,7 @@
         both = [jnp.dot(tok[k], wq[...], preferred_element_type=F32) for k in ks]
         for k, a in zip(ks, both):
             for h in range(heads):
-                qs[k * heads + h] = turned(a[:, lanes(h)])
+                qs[k * heads + h] = turned(a[:, lanes(h)], scale)
 
     cos_at, sin_at = cos_base[pl.ds(sp, 1)], sin_base[pl.ds(sp, 1)]
     sign = jnp.where(iota(cos.shape, 1) < HEAD_DIM // 2, -1.0, 1.0)
@@ -395,7 +396,7 @@
         qp[step, :, sl] = moved.reshape(FAR, FAR, HEAD_DIM)
         k = kn[h, near, lanes(0)]
         v = kn[h, near, lanes(1)]
-        sc = dot_t(moved, k) * scale + bias1[jb, g]
+        sc = dot_t(moved, k) + bias1[jb, g]
         m = jnp.max(sc, axis=1, keepdims=True)
         p = jnp.exp2(sc - m)
         l = jnp.sum(p, axis=1, keepdims=True)
@@ -425,11 +426,11 @@
             q = qp[slot, sel].reshape(flat)
             k4 = kp[h, sel, near, :HEAD_DIM].reshape(-1, HEAD_DIM)
             v4 = kp[h, sel, near, HEAD_DIM:].reshape(-1, HEAD_DIM)
-            s4 = dot_t(q, k4) * scale + bias4[jb]
+            s4 = dot_t(q, k4) + bias4[jb]
             b16 = bias16[jb]
             s16 = jnp.concatenate(
                 [
-                    dot_t(qp[slot, group * per + i], kp[h, group * per + i, whole, :HEAD_DIM]) * scale + b16
+                    dot_t(qp[slot, group * per + i], kp[h, group * per + i, whole, :HEAD_DIM]) + b16
                     for i in range(per)
                 ],
                 axis=0,
@@ -607,7 +608,8 @@
     halo(1)
     gather_ends(1)
     close_outer(1, 0)
-    collect(0, 1, 3)
+    collect(0, 1)
+    collect(0, 3)
     attend_far(1, 0)
     relay(0, 2)
     collect_mine(1)

time: 64 us -> 64 us (level); the launches traced: 63.5 us -> 62.8 us
    pallas_call x1, Pallas kernels: 61.5 us -> 60.8 us  [layer(): pl.pallas_call(functools.partial(layer_kernel, nsp), in_specs=[hbm] * 7 +...]
where the time goes in v7:
time: 64 us; the launch traced here: 62.8 us
  Pallas kernels  62 us (97%)
  between operations  0.82 us (1%)
    pallas_call x1, Pallas kernels, layer(): pl.pallas_call(functools.partial(layer_kernel, nsp), in_specs=[hbm] * 7 +...  60.8 us

profile of v7, /device:TPU:160, one launch (start us, length us, event | category | flops | bytes accessed | tf_op | source)
XLA Modules:
  0.0 62.8 jit_solution(276927676791592883)
XLA Ops:
  0.6 60.8 %layer.1 = (bf16[4,384,512]{2,1,0:T(8,128)(2,1)S(1)}, f32[4,2,384]{2,1,0:T(2,128)S(1)}) custom-call(bf16[4,384,2048]{2,1,0:T(8,128)(2,1)} %tok_h.1, bf16[2048,256]{1,0:T(8,128)(2,1)} %wq_h.1, bf16[2048,256]{1,0:T(8,128)(2,1)} %wk_h.1, bf16[2048,256]{1,0:T(8,128)(2,1)} %wv_h.1, bf16[1024,512]{1,0:T(8,128)(2,1)} %wo_h.1, f32[384,128]{1,0:T(8,128)} %constant.8.clone.cos_h, ...), custom_call_target="tpu_custom_call" | custom-call | tf_op jit(solution)/shard_map/layer/pallas_call | solution.py:677
  61.4 1.2 %store.1 = (bf16[4,384,512]{2,1,0:T(8,128)(2,1)}, f32[4,2,384]{2,1,0:T(2,128)}) custom-call(bf16[4,384,512]{2,1,0:T(8,128)(2,1)S(1)} %get-tuple-element.4.mixed, f32[4,2,384]{2,1,0:T(2,128)S(1)} %get-tuple-element.5.logs), custom_call_target="tpu_custom_call" | custom-call | tf_op jit(solution)/shard_map/store/pallas_call | solution.py:734
